TPU v7x, 32 devices: a whole 2x2x4 slice. The times are simulated.
32 devices in a mesh: grp: 2 (over y), sp: 4 (over z), tp: 4 (over x, core).
Axes of the slice: x: 2, y: 2, z: 4, core: 2. Of those that a mesh axis runs over, the one named last changes fastest.
Arguments:
- tokens: bfloat16 [2048, 2048], P(('grp', 'sp'), 'tp'), parts along dimension 0, may hold values from -6 to 6
- norm_gain: float32 [2048], replicated, may hold values from 0.1 to 1.9
- ret_query_weight: bfloat16 [2048, 256], P('sp', 'tp'), may hold values from -0.125 to 0.125
- ret_key_weight: bfloat16 [2048, 256], P('sp', 'tp'), may hold values from -0.125 to 0.125
- ret_value_weight: bfloat16 [2048, 512], P('sp', 'tp'), may hold values from -0.125 to 0.125
- fox_query_weight: bfloat16 [2048, 512], P('sp', 'tp'), may hold values from -8 to 8
- fox_key_weight: bfloat16 [2048, 512], P('sp', 'tp'), may hold values from -0.125 to 0.125
- fox_value_weight: bfloat16 [2048, 512], P('sp', 'tp'), may hold values from -0.125 to 0.125
- ret_decay: float32 [8], P('tp'), may hold values from -1 to 0, as said below
- ret_state: float32 [16, 32, 64], P(('grp', 'tp')), parts along dimension 0, may hold values from -64 to 64
- head_norm_gain: float32 [512], P('tp'), may hold values from 0.1 to 1.9
- fox_gates: float32 [2048, 8], P('grp', 'tp'), parts along dimension 0, may hold values from -3072 to 0, as said below
- ret_out_weight: bfloat16 [512, 2048], P('tp', 'sp'), may hold values from -0.1875 to 0.1875
- fox_out_weight: bfloat16 [512, 2048], P('tp', 'sp'), may hold values from -1 to 1
Outputs:
- mixed: bfloat16 [2048, 2048], P(('grp', 'sp', 'tp')), parts along dimension 0
There are 2 independent parts, one for each index of `grp`. A program takes and returns all parts, laid end to end along the dimension named above; an argument that names none is the same for every part. Nothing has to cross between parts.
Inputs may be any that keep to these rules, and one draw needn't show every extreme that they name: `ret_decay`: each head's log decay is negative. `fox_gates`: along the positions each head's column never rises.
All inputs are finite; a program needn't handle non-finite values.
Results may differ from a plain program's by a relative error of at most 0.015.
The roundings to bfloat16 on the way count: a program that leaves them out, or rounds other values in their place, can miss the bound.
Values may be sent and summed in bfloat16 or wider, within the bound.
A program may use at most 64 MiB of HBM per device.

v0:
```python
import jax
import jax.numpy as jnp
from jax import lax
from jax.sharding import PartitionSpec as P

epsilon = 1e-06
highest = lax.Precision.HIGHEST


def head_group_norm(joined_output, norm_gains):
    center = joined_output - jnp.mean(joined_output, axis=-1, keepdims=True)
    spread = jnp.mean(center * center, axis=-1, keepdims=True)
    normal = (
        center
        * lax.rsqrt(spread + epsilon)
        * norm_gains.reshape(joined_output.shape[1], joined_output.shape[2])
    )
    return normal.reshape(joined_output.shape[0], -1).astype(jnp.bfloat16)


def softmax_update(
    current,
    query_heads,
    query_gates,
    query_pos,
    key_block,
    value_block,
    gate_block,
    key_pos,
    score_scale,
):
    top_now, total_now, weighted = current
    logits = (
        jnp.einsum("qhd,khd->hqk", query_heads, key_block, preferred_element_type=jnp.float32)
        * score_scale
    )
    logits = logits + query_gates[:, :, None] - gate_block[:, None, :]
    logits = jnp.where(key_pos[None, None, :] <= query_pos[None, :, None], logits, -jnp.inf)
    top_new = jnp.maximum(top_now, jnp.max(logits, axis=-1))
    weights_new = jnp.exp(logits - top_new[:, :, None])
    rescale = jnp.exp(top_now - top_new)
    total_new = total_now * rescale + jnp.sum(weights_new, axis=-1)
    weighted_new = weighted * rescale[:, :, None] + jnp.einsum(
        "hqk,khd->hqd",
        weights_new.astype(jnp.bfloat16),
        value_block,
        preferred_element_type=jnp.float32,
    )
    return (top_new, total_new, weighted_new)


def local(
    tokens,
    norm_gain,
    ret_query_weight,
    ret_key_weight,
    ret_value_weight,
    fox_query_weight,
    fox_key_weight,
    fox_value_weight,
    ret_decay,
    ret_state,
    head_norm_gain,
    fox_gates,
    ret_out_weight,
    fox_out_weight,
):
    sequence_length = tokens.shape[0]
    gathered = lax.all_gather(tokens, "tp", axis=1, tiled=True)
    widened = gathered.astype(jnp.float32)
    normed = (
        widened
        * lax.rsqrt(jnp.mean(widened * widened, axis=-1, keepdims=True) + epsilon)
        * norm_gain
    ).astype(jnp.bfloat16)
    portions = (
        lax.all_gather(ret_query_weight, "sp", axis=0, tiled=True),
        lax.all_gather(ret_key_weight, "sp", axis=0, tiled=True),
        lax.all_gather(ret_value_weight, "sp", axis=0, tiled=True),
        lax.all_gather(fox_query_weight, "sp", axis=0, tiled=True),
        lax.all_gather(fox_key_weight, "sp", axis=0, tiled=True),
        lax.all_gather(fox_value_weight, "sp", axis=0, tiled=True),
    )
    sums = tuple(
        (jnp.dot(normed, portion, preferred_element_type=jnp.float32) for portion in portions)
    )
    ret_query, ret_key, ret_value, fox_query, fox_key, fox_value = [
        result.astype(jnp.bfloat16) for result in sums
    ]
    ret_heads = ret_decay.shape[0]
    key_size = ret_query.shape[1] // ret_heads
    value_size = ret_value.shape[1] // ret_heads
    place = lax.axis_index("sp")
    offset = place * sequence_length
    queries = ret_query.astype(jnp.float32).reshape(sequence_length, ret_heads, key_size)
    keys_local = ret_key.astype(jnp.float32).reshape(
        sequence_length, ret_heads, key_size
    ) * key_size ** (-0.5)
    values_local = ret_value.astype(jnp.float32).reshape(sequence_length, ret_heads, value_size)
    positions = jnp.arange(sequence_length, dtype=jnp.float32)
    spread = positions[:, None] - positions[None, :]
    within = jnp.where(
        spread[None] >= 0, jnp.exp(jnp.maximum(spread, 0.0)[None] * ret_decay[:, None, None]), 0.0
    )
    leading = jnp.exp((positions + 1.0)[:, None] * ret_decay[None, :])
    trailing = jnp.exp((sequence_length - 1.0 - positions)[:, None] * ret_decay[None, :])
    scores = jnp.einsum("ihd,jhd->hij", queries, keys_local, precision=highest) * within
    inner_value = jnp.einsum("hij,jhe->ihe", scores, values_local, precision=highest)
    summary = jnp.einsum(
        "jhd,jhe->hde", keys_local * trailing[:, :, None], values_local, precision=highest
    )
    portion = lax.all_gather(summary[None], "sp", axis=0, tiled=True)
    shard_ids = jnp.arange(portion.shape[0], dtype=jnp.int32)
    distance = jnp.maximum(place - shard_ids - 1, 0).astype(jnp.float32) * sequence_length
    weight = jnp.where(
        (shard_ids < place)[:, None], jnp.exp(distance[:, None] * ret_decay[None, :]), 0.0
    )
    before = jnp.einsum("sh,shde->hde", weight, portion, precision=highest)
    entering = jnp.exp(offset.astype(jnp.float32) * ret_decay)[:, None, None] * ret_state + before
    carried_state = (
        jnp.einsum("ihd,hde->ihe", queries, entering, precision=highest) * leading[:, :, None]
    )
    retention_mixed = head_group_norm(inner_value + carried_state, head_norm_gain)
    fox_heads = fox_gates.shape[1]
    head_size = fox_query.shape[1] // fox_heads
    score_scale = head_size ** (-0.5)
    starting = (
        jnp.full((fox_heads, sequence_length), -1e30, jnp.float32),
        jnp.zeros((fox_heads, sequence_length), jnp.float32),
        jnp.zeros((fox_heads, sequence_length, head_size), jnp.float32),
    )
    query_heads = fox_query.reshape(sequence_length, fox_heads, head_size)
    own_gates = lax.dynamic_slice_in_dim(fox_gates, offset, sequence_length, 0).T
    query_pos = offset + jnp.arange(sequence_length, dtype=jnp.int32)
    last_query = offset + sequence_length - 1

    def attend(running, portion, first_key):
        key_rows, value_rows = portion
        count = key_rows.shape[0]
        block_rows = next(
            (candidate for candidate in (2048, 1024, 512) if count % candidate == 0), count
        )

        def advance(state_now, number):
            key_start = first_key + number * block_rows

            def compute(current):
                key_block = lax.dynamic_slice_in_dim(
                    key_rows, number * block_rows, block_rows, 0
                ).reshape(block_rows, fox_heads, head_size)
                value_block = lax.dynamic_slice_in_dim(
                    value_rows, number * block_rows, block_rows, 0
                ).reshape(block_rows, fox_heads, head_size)
                gate_block = lax.dynamic_slice_in_dim(fox_gates, key_start, block_rows, 0).T
                key_pos = key_start + jnp.arange(block_rows, dtype=jnp.int32)
                return softmax_update(
                    current,
                    query_heads,
                    own_gates,
                    query_pos,
                    key_block,
                    value_block,
                    gate_block,
                    key_pos,
                    score_scale,
                )

            def unchanged(current):
                return current

            return (lax.cond(key_start <= last_query, compute, unchanged, state_now), None)

        finished, _ = lax.scan(advance, running, jnp.arange(count // block_rows, dtype=jnp.int32))
        return finished

    top_final, total_final, weighted_final = attend(
        starting,
        (
            lax.all_gather(fox_key, "sp", axis=0, tiled=True),
            lax.all_gather(fox_value, "sp", axis=0, tiled=True),
        ),
        jnp.int32(0),
    )
    fox_mix = (
        jnp.transpose(weighted_final / total_final[:, :, None], (1, 0, 2))
        .reshape(sequence_length, fox_heads * head_size)
        .astype(jnp.bfloat16)
    )
    ret_full, fox_full = (
        lax.all_gather(ret_out_weight, "sp", axis=1, tiled=True),
        lax.all_gather(fox_out_weight, "sp", axis=1, tiled=True),
    )
    return lax.psum_scatter(
        (
            jnp.dot(retention_mixed, ret_full, preferred_element_type=jnp.float32)
            + jnp.dot(fox_mix, fox_full, preferred_element_type=jnp.float32)
        ).astype(jnp.bfloat16),
        "tp",
        scatter_dimension=0,
        tiled=True,
    )


def solution(mesh):
    placed = (
        P(("grp", "sp"), "tp"),
        P(),
        P("sp", "tp"),
        P("sp", "tp"),
        P("sp", "tp"),
        P("sp", "tp"),
        P("sp", "tp"),
        P("sp", "tp"),
        P("tp"),
        P(("grp", "tp"), None, None),
        P("tp"),
        P("grp", "tp"),
        P("tp", "sp"),
        P("tp", "sp"),
    )
    return jax.shard_map(
        local, mesh=mesh, in_specs=placed, out_specs=P(("grp", "sp", "tp"), None), check_vma=False
    )
```

profile of v0, /device:TPU:24, one launch (start us, length us, event | category | flops | bytes accessed | tf_op | source)
XLA Modules:
  0.0 226.0 jit_solution(7468177820457589616)
XLA Ops:
  6.5 0.0 all-gather.3.cloned.1.call-start
  6.6 0.7 all-gather.3.cloned.1.call-update
  7.3 0.0 reduce-scatter.2.cloned.1.call-start
  7.3 0.6 iota_add_fusion
  8.0 0.7 fusion.11
  8.7 14.8 %all_gather.38 = bf16[2048,64]{0,1:T(8,128)(2,1)} all-gather(bf16[512,64]{0,1:T(8,128)(2,1)} %param.18), channel_id=1, replica_groups=mesh['grp'=2,'sp'=4,'tp'=4] {'sp'}, dimensions={0}, use_global_device_ids=true | all-gather | bytes 327680 | tf_op jit(solution)/shard_map/all_gather | solution.py:77
  23.5 15.0 %all_gather.37 = bf16[2048,128]{1,0:T(8,128)(2,1)S(1)} all-gather(bf16[512,128]{1,0:T(8,128)(2,1)} %param.20), channel_id=1, replica_groups=mesh['grp'=2,'sp'=4,'tp'=4] {'sp'}, dimensions={0}, use_global_device_ids=true | all-gather | bytes 655360 | tf_op jit(solution)/shard_map/all_gather | solution.py:79
  38.5 1.3 dynamic-slice_bitcast_fusion
  39.8 0.7 select_bitcast_fusion
  40.5 15.3 %all_gather.39 = bf16[2048,64]{0,1:T(8,128)(2,1)} all-gather(bf16[512,64]{0,1:T(8,128)(2,1)} %param.19), channel_id=1, replica_groups=mesh['grp'=2,'sp'=4,'tp'=4] {'sp'}, dimensions={0}, use_global_device_ids=true | all-gather | bytes 327680 | tf_op jit(solution)/shard_map/all_gather | solution.py:78
  55.8 0.7 copy.21
  56.5 1.3 mul.215
  57.8 0.1 fusion.10
  57.9 0.0 copy-done.3
  57.9 16.1 %all_gather.42 = bf16[2048,128]{1,0:T(8,128)(2,1)S(1)} all-gather(bf16[512,128]{1,0:T(8,128)(2,1)S(1)} %copy-done.3), channel_id=1, replica_groups=mesh['grp'=2,'sp'=4,'tp'=4] {'sp'}, dimensions={0}, use_global_device_ids=true | all-gather | bytes 655360 | tf_op jit(solution)/shard_map/all_gather | solution.py:80
  73.9 0.0 copy-done.4
  73.9 16.2 %all_gather.43 = bf16[2048,128]{1,0:T(8,128)(2,1)S(1)} all-gather(bf16[512,128]{1,0:T(8,128)(2,1)S(1)} %copy-done.4), channel_id=1, replica_groups=mesh['grp'=2,'sp'=4,'tp'=4] {'sp'}, dimensions={0}, use_global_device_ids=true | all-gather | bytes 655360 | tf_op jit(solution)/shard_map/all_gather | solution.py:81
  90.2 0.0 copy-done.5
  90.2 16.0 %all_gather.45 = bf16[2048,128]{1,0:T(8,128)(2,1)S(1)} all-gather(bf16[512,128]{1,0:T(8,128)(2,1)S(1)} %copy-done.5), channel_id=1, replica_groups=mesh['grp'=2,'sp'=4,'tp'=4] {'sp'}, dimensions={0}, use_global_device_ids=true | all-gather | bytes 655360 | tf_op jit(solution)/shard_map/all_gather | solution.py:82
  106.2 0.0 copy-done.6
  106.2 15.2 %all_gather.41 = bf16[128,2048]{1,0:T(8,128)(2,1)S(1)} all-gather(bf16[128,512]{1,0:T(8,128)(2,1)S(1)} %copy-done.6), channel_id=1, replica_groups=mesh['grp'=2,'sp'=4,'tp'=4] {'sp'}, dimensions={1}, use_global_device_ids=true | all-gather | bytes 655360 | tf_op jit(solution)/shard_map/all_gather | solution.py:190
  121.3 15.7 %all_gather.47 = bf16[128,2048]{1,0:T(8,128)(2,1)S(1)} all-gather(bf16[128,512]{1,0:T(8,128)(2,1)} %param.29), channel_id=1, replica_groups=mesh['grp'=2,'sp'=4,'tp'=4] {'sp'}, dimensions={1}, use_global_device_ids=true | all-gather | bytes 655360 | tf_op jit(solution)/shard_map/all_gather | solution.py:191
  137.1 0.0 copy-done.8
  137.1 0.6 multiply_exponential_fusion.1
  137.7 0.8 exponential_multiply_fusion
  138.4 0.0 all-gather.3.cloned.1.call-done
  138.4 0.0 copy-start
  138.5 1.6 fusion.5
  140.1 0.0 copy-start.9
  140.1 0.0 copy-start.1
  140.1 0.0 copy-start.14
  140.1 1.8 convolution_convert_fusion.4
  141.9 0.0 copy-start.2
  141.9 1.3 convolution_convert_fusion.3
  143.2 0.0 copy-start.7
  143.3 0.2 fusion.14
  143.4 13.6 %all-gather = f32[8,32,64]{2,1,0:T(8,128)S(1)} all-gather(f32[2,32,64]{2,1,0:T(8,128)S(1)} %fusion.14), channel_id=2, replica_groups=mesh['grp'=2,'sp'=4,'tp'=4] {'sp'}, dimensions={0}, use_global_device_ids=true | all-gather | bytes 81920 | tf_op jit(solution)/shard_map/all_gather | solution.py:112
  157.1 0.0 copy-done.9
  157.1 0.4 fusion.12
  157.5 0.5 convolution_convert_fusion.5
  158.0 0.5 convolution_multiply_fusion
  158.5 0.3 fusion.9
  158.9 0.4 fusion.28
  159.4 0.5 convolution_convert_fusion.1
  159.9 13.9 %all_gather.44 = bf16[1024,128]{1,0:T(8,128)(2,1)S(1)} all-gather(bf16[256,128]{1,0:T(8,128)(2,1)S(1)} %convolution_convert_fusion.1), channel_id=1, replica_groups=mesh['grp'=2,'sp'=4,'tp'=4] {'sp'}, dimensions={0}, use_global_device_ids=true | all-gather | bytes 327680 | tf_op jit(solution)/shard_map/all_gather | solution.py:179
  173.7 0.5 convolution_convert_fusion
  174.2 0.0 copy-start.13
  174.3 13.9 %all_gather.46 = bf16[1024,128]{1,0:T(8,128)(2,1)S(1)} all-gather(bf16[256,128]{1,0:T(8,128)(2,1)S(1)} %convolution_convert_fusion), channel_id=1, replica_groups=mesh['grp'=2,'sp'=4,'tp'=4] {'sp'}, dimensions={0}, use_global_device_ids=true | all-gather | bytes 327680 | tf_op jit(solution)/shard_map/all_gather | solution.py:180
  188.1 0.1 multiply_convert_fusion
  188.2 0.5 convolution_convert_fusion.2
  188.7 0.0 copy-done.10
  188.7 0.0 copy-done.13
  188.7 2.6 %conditional.1 = ((f32[2,256]{1,0:T(2,128)S(1)}, f32[2,256,64]{1,2,0:T(8,128)S(1)})) conditional(s32[]{:T(128)} %convert_element_type.74, (f32[2,256]{1,0:T(2,128)S(1)}, f32[2,256,64]{1,2,0:T(8,128)S(1)}) %tuple.25, (s32[]{:T(128)}, s32[256]{0:T(256)S(1)}, bf16[256,128]{1,0:T(8,128)(2,1)S(1)}, bf16[1024,128]{1,0:T(8,128)(2,1)S(1)}, ...), branch_computations={%region_3.4_spmd, %region_4.0_spmd} | conditional | flops 139265792 | bytes 8885276 | solution.py:171
  188.8 0.1 copy.20
  188.9 0.1 copy.18
  189.0 0.2 iota_compare_fusion
  189.3 0.1 copy.19
  189.4 0.8 fusion.27
  190.2 0.5 fusion.1
  190.8 0.6 convolution_add_fusion
  191.4 0.5 fusion.29
  191.8 1.4 fusion.4
  193.2 0.0 reduce-scatter.2.cloned.1.call-update
  193.3 25.9 %reduce-scatter.2.cloned.1.call-done = bf16[64,2048]{1,0:T(8,128)(2,1)} async-done(((bf16[256,2048]{1,0:T(8,128)(2,1)}), bf16[64,2048]{1,0:T(8,128)(2,1)}) %reduce-scatter.2.cloned.1.call-update) | async-done | bytes 262160 | tf_op jit(solution)/shard_map/reduce_scatter | solution.py:193
  (28 shorter events, 0.2 us)
Async XLA Ops:
  6.5 51.3 %copy-start.3 = (bf16[512,128]{1,0:T(8,128)(2,1)S(1)}, bf16[512,128]{1,0:T(8,128)(2,1)}, u32[]{:S(2)}) copy-start(bf16[512,128]{1,0:T(8,128)(2,1)} %param.21) | copy-start | bytes 393220
  6.5 67.4 %copy-start.4 = (bf16[512,128]{1,0:T(8,128)(2,1)S(1)}, bf16[512,128]{1,0:T(8,128)(2,1)}, u32[]{:S(2)}) copy-start(bf16[512,128]{1,0:T(8,128)(2,1)} %param.22) | copy-start | bytes 393220
  6.5 83.7 %copy-start.5 = (bf16[512,128]{1,0:T(8,128)(2,1)S(1)}, bf16[512,128]{1,0:T(8,128)(2,1)}, u32[]{:S(2)}) copy-start(bf16[512,128]{1,0:T(8,128)(2,1)} %param.23) | copy-start | bytes 393220
  6.5 99.6 %copy-start.6 = (bf16[128,512]{1,0:T(8,128)(2,1)S(1)}, bf16[128,512]{1,0:T(8,128)(2,1)}, u32[]{:S(2)}) copy-start(bf16[128,512]{1,0:T(8,128)(2,1)} %param.28) | copy-start | bytes 393220
  6.5 131.9 %all-gather.3.cloned.1.call-start = ((), (), s32[]{:S(2)}) async-start(), calls=%async_computation.1 | async-start | bytes 1310720 | tf_op jit(solution)/shard_map/all_gather | solution.py:69
  7.3 211.9 %reduce-scatter.2.cloned.1.call-start = ((), (), s32[]{:S(2)}) async-start(), calls=%async_computation.2 | async-start | bytes 1310720 | tf_op jit(solution)/shard_map/reduce_scatter | solution.py:193
  38.5 98.6 %copy-start.8 = (f32[2]{0:T(128)S(1)}, f32[2]{0:T(128)}, u32[]{:S(2)}) copy-start(f32[2]{0:T(128)} %param.24) | copy-start | bytes 28
  138.4 3.5 %copy-start = (bf16[256,2048]{1,0:T(8,128)(2,1)S(1)}, bf16[256,2048]{1,0:T(8,128)(2,1)}, u32[]{:S(2)}) copy-start(bf16[256,2048]{1,0:T(8,128)(2,1)} %all-gather.3.cloned.1.call-done) | copy-start | bytes 3145732
  140.1 17.0 %copy-start.9 = (f32[4,2,1,1]{0,2,3,1:T(1,128)S(1)}, f32[4,2,1,1]{0,2,3,1:T(1,128)}, u32[]{:S(2)}) copy-start(f32[4,2,1,1]{0,2,3,1:T(1,128)} %copy.21) | copy-start | bytes 100
  140.1 17.4 %copy-start.1 = (bf16[2048,64]{0,1:T(8,128)(2,1)S(1)}, bf16[2048,64]{0,1:T(8,128)(2,1)}, u32[]{:S(2)}) copy-start(bf16[2048,64]{0,1:T(8,128)(2,1)} %all_gather.38) | copy-start | bytes 786436
  140.1 17.4 %copy-start.14 = (f32[2048]{0:T(1024)S(1)}, f32[2048]{0:T(1024)}, u32[]{:S(2)}) copy-start(f32[2048]{0:T(1024)} %param.17) | copy-start | bytes 24580
  141.9 16.1 %copy-start.2 = (pred[256,256]{1,0:T(8,128)(4,1)S(1)}, pred[256,256]{1,0:T(8,128)(4,1)}, u32[]{:S(2)}) copy-start(pred[256,256]{1,0:T(8,128)(4,1)} %fusion.11) | copy-start | bytes 196612
  143.2 15.3 %copy-start.7 = (f32[2,32,64]{2,1,0:T(8,128)S(1)}, f32[2,32,64]{2,1,0:T(8,128)}, u32[]{:S(2)}) copy-start(f32[2,32,64]{2,1,0:T(8,128)} %param.25) | copy-start | bytes 49156
  143.3 15.3 %copy-start.12 = (f32[2]{0:T(128)S(1)}, f32[2]{0:T(128)}, u32[]{:S(2)}) copy-start(f32[2]{0:T(128)} %multiply_exponential_fusion.1) | copy-start | bytes 28
  159.9 28.3 %copy-start.11 = (f32[2,64]{1,0:T(2,128)S(1)}, f32[2,64]{1,0:T(2,128)}, u32[]{:S(2)}) copy-start(f32[2,64]{1,0:T(2,128)} %mul.215) | copy-start | bytes 1540
  174.2 14.5 %copy-start.10 = (f32[2,256]{1,0:T(2,128)S(1)}, f32[2,256]{1,0:T(2,128)}, u32[]{:S(2)}) copy-start(f32[2,256]{1,0:T(2,128)} %dynamic-slice_bitcast_fusion) | copy-start | bytes 6148
  174.2 14.5 %copy-start.13 = (f32[1024,2]{0,1:T(2,128)S(1)}, f32[1024,2]{0,1:T(2,128)}, u32[]{:S(2)}) copy-start(f32[1024,2]{0,1:T(2,128)} %param.27) | copy-start | bytes 24580
Sparse Core Ops, SparseCore 0:
  8.9 17.6 all-gather.2
  193.4 25.7 reduce-scatter.1
where the time goes:
time: 228 us; the launch traced here: 226 us
  blocking collectives  166 us (73%)
  waiting for transfers between devices  26.6 us (12%)
  between operations  13.7 us (6%)
  matrix products  10.1 us (4%)
  other arithmetic  5.95 us (3%)
  local copies, waits for them, and re-layouts  3.75 us (2%)
    reduce_scatter x1, waiting for transfers between devices, local(): lax.psum_scatter((jnp.dot(retention_mixed, ret_full, preferred_element_ty...  25.9 us
    all_gather x1, blocking collectives, local(): lax.all_gather(fox_key_weight, 'sp', axis=0, tiled=True)  16.2 us
    all_gather x1, blocking collectives, local(): lax.all_gather(fox_query_weight, 'sp', axis=0, tiled=True)  16.1 us
    all_gather x1, blocking collectives, local(): lax.all_gather(fox_value_weight, 'sp', axis=0, tiled=True)  16 us
    all_gather x1, blocking collectives, local(): lax.all_gather(fox_out_weight, 'sp', axis=1, tiled=True)  15.7 us
    all_gather x1, blocking collectives, local(): lax.all_gather(ret_key_weight, 'sp', axis=0, tiled=True)  15.3 us
    all_gather x1, blocking collectives, local(): lax.all_gather(ret_out_weight, 'sp', axis=1, tiled=True)  15.2 us
    all_gather x1, blocking collectives, local(): lax.all_gather(ret_value_weight, 'sp', axis=0, tiled=True)  15 us
  transfers between devices with their start and end apart: 2, of which 1 were waited for; matrix products, arithmetic and copies ran while one was open for 3% of the time, Pallas kernels for 0%

commit v1 on v0

v1 whole, which is shorter than its diff:
```python
import functools

import jax
import jax.numpy as jnp
from jax import lax
from jax.experimental import pallas as pl
from jax.experimental.pallas import tpu as pltpu
from jax.sharding import PartitionSpec as P

epsilon = 1e-06
highest = lax.Precision.HIGHEST
NT = (((1,), (1,)), ((), ()))
TN = (((0,), (0,)), ((), ()))


def rdma(src, dst, send_sem, recv_sem, **target):
    return pltpu.make_async_remote_copy(
        src_ref=src,
        dst_ref=dst,
        send_sem=send_sem,
        recv_sem=recv_sem,
        device_id=target,
        device_id_type=pl.DeviceIdType.MESH,
    )


class LineGather:
    def __init__(self, own, buf, sems, n, n_grp, me, g, chunks):
        self.own, self.buf, self.n, self.n_grp, self.me, self.g = own, buf, n, n_grp, me, g
        self.up, self.down, self.zr, self.ys, self.yr, self.loc = sems
        self.rows = own.shape[0]
        self.part = self.rows // n_grp
        self.chunks = chunks
        self.step = self.part // chunks

    def piece(self, part, src, c):
        start = pl.multiple_of(src * self.rows + part * self.part + c * self.step, self.step)
        return self.buf.at[pl.ds(start, self.step)]

    def own_piece(self, c):
        start = pl.multiple_of(self.g * self.part + c * self.step, self.step)
        return self.own.at[pl.ds(start, self.step)]

    def hop(self, sems, to, src, c, first=False):
        here = self.own_piece(c) if first else self.piece(self.g, src, c)
        at = src * self.chunks + c
        return rdma(here, self.piece(self.g, src, c), sems.at[at], self.zr.at[at], sp=to)

    def side(self, d, src, c):
        at = ((d - 1) * self.n + src) * self.chunks + c
        here = self.piece(self.g, src, c)
        return rdma(here, here, self.ys.at[at], self.yr.at[at], grp=lax.rem(self.g + d, self.n_grp))

    def side_in(self, d, src, c):
        at = ((d - 1) * self.n + src) * self.chunks + c
        part = lax.rem(self.g + self.n_grp - d, self.n_grp)
        here = self.piece(part, src, c)
        return rdma(here, here, self.ys.at[at], self.yr.at[at], grp=part)

    def local(self):
        start = pl.multiple_of(self.me * self.rows, self.rows)
        return pltpu.make_async_copy(self.own, self.buf.at[pl.ds(start, self.rows)], self.loc)

    def start(self):
        me, n = self.me, self.n
        for c in range(self.chunks):

            @pl.when(me + 1 < n)
            def _():
                self.hop(self.up, me + 1, me, c, True).start()

            @pl.when(me >= 1)
            def _():
                self.hop(self.down, me - 1, me, c, True).start()

        self.local().start()

    def relay(self):
        me, n = self.me, self.n

        def step(k, _):
            for c in range(self.chunks):
                for src, sems, to in ((me - k, self.up, me + 1), (me + k, self.down, me - 1)):

                    @pl.when((src >= 0) & (src < n))
                    def _(src=src, sems=sems, to=to):
                        self.hop(sems, me, src, c).wait_recv()

                        @pl.when((to >= 0) & (to < n))
                        def _():
                            self.hop(sems, to, src, c).start()

                        for d in range(1, self.n_grp):
                            self.side(d, src, c).start()

            return 0

        lax.fori_loop(1, n, step, 0)

    def arrive(self):
        self.local().wait()

        def step(k, _):
            src = lax.rem(self.me + k, self.n)
            for c in range(self.chunks):
                for d in range(1, self.n_grp):
                    self.side_in(d, src, c).wait_recv()
            return 0

        lax.fori_loop(1, self.n, step, 0)

    def finish(self):
        me, n = self.me, self.n

        def step(src, _):
            for c in range(self.chunks):

                @pl.when((src <= me) & (me + 1 < n))
                def _():
                    self.hop(self.up, me, src, c).wait_send()

                @pl.when((src >= me) & (me >= 1))
                def _():
                    self.hop(self.down, me, src, c).wait_send()

                @pl.when(src != me)
                def _():
                    for d in range(1, self.n_grp):
                        self.side(d, src, c).wait_send()

            return 0

        lax.fori_loop(0, n, step, 0)


def kernel(
    size,
    tok_ref,
    gain_ref,
    w_ref,
    decay_ref,
    state_ref,
    hgain_ref,
    gates_ref,
    gates_t_ref,
    wout_ref,
    out_ref,
    tok_buf,
    w_buf,
    wout_buf,
    norm_buf,
    proj_buf,
    kv_buf,
    sum_buf,
    mix_buf,
    rs_send,
    rs_buf,
    tok_s,
    tok_r,
    tok_loc,
    kv_s,
    kv_r,
    sum_s,
    sum_r,
    rs_s,
    rs_r,
    *gather_sems,
):
    n, n_tp, n_grp, hr, dk, vd, fh, fd, chunks, out_chunks = size
    me, t, g = lax.axis_index("sp"), lax.axis_index("tp"), lax.axis_index("grp")
    rows = tok_ref.shape[0]
    feats = tok_ref.shape[1]
    weights = LineGather(w_ref, w_buf, gather_sems[:6], n, n_grp, me, g, chunks)
    outs = LineGather(wout_ref, wout_buf, gather_sems[6:], n, n_grp, me, g, out_chunks)

    barrier = pltpu.get_barrier_semaphore()

    def greet(**target):
        pl.semaphore_signal(barrier, inc=1, device_id=target, device_id_type=pl.DeviceIdType.MESH)

    has_up, has_down = me + 1 < n, me >= 1
    for d in range(1, n_tp):
        greet(tp=lax.rem(t + d, n_tp))
    for d in range(1, n_grp):
        greet(grp=lax.rem(g + d, n_grp))

    @pl.when(has_up)
    def _():
        greet(sp=me + 1)

    @pl.when(has_down)
    def _():
        greet(sp=me - 1)

    count = n_tp - 1 + n_grp - 1 + has_up.astype(jnp.int32) + has_down.astype(jnp.int32)
    pl.semaphore_wait(barrier, count)

    weights.start()

    def tok_copy(d):
        return rdma(tok_ref, tok_buf.at[t], tok_s.at[d - 1], tok_r.at[d - 1], tp=lax.rem(t + d, n_tp))

    def tok_in(d):
        src = lax.rem(t + n_tp - d, n_tp)
        return rdma(tok_ref, tok_buf.at[src], tok_s.at[d - 1], tok_r.at[d - 1], tp=src)

    tok_local = pltpu.make_async_copy(tok_ref, tok_buf.at[t], tok_loc)
    for d in range(1, n_tp):
        tok_copy(d).start()
    tok_local.start()

    weights.relay()
    outs.start()

    tok_local.wait()
    for d in range(1, n_tp):
        tok_in(d).wait_recv()
    squares = jnp.zeros((rows, 1), jnp.float32)
    for i in range(n_tp):
        part = tok_buf[i].astype(jnp.float32)
        squares = squares + jnp.sum(part * part, axis=-1, keepdims=True)
    scale = lax.rsqrt(squares * (1.0 / (n_tp * feats)) + epsilon)
    for i in range(n_tp):
        part = tok_buf[i].astype(jnp.float32)
        cols = slice(i * feats, (i + 1) * feats)
        norm_buf[:, cols] = (part * scale * gain_ref[:, cols]).astype(jnp.bfloat16)

    outs.relay()
    weights.arrive()

    fox_kv = hr * (2 * dk + vd) + fh * fd
    kv_width = 2 * fh * fd
    result = jnp.dot(norm_buf[...], w_buf[...], preferred_element_type=jnp.float32)
    proj_buf[...] = result.astype(jnp.bfloat16)
    kv_buf[me] = proj_buf[:, fox_kv : fox_kv + kv_width]

    def kv_copy(src):
        return rdma(kv_buf.at[src], kv_buf.at[src], kv_s.at[src], kv_r.at[src], sp=jnp.minimum(me + 1, n - 1))

    def sum_copy(src):
        return rdma(sum_buf.at[src], sum_buf.at[src], sum_s.at[src], sum_r.at[src], sp=jnp.minimum(me + 1, n - 1))

    @pl.when(has_up)
    def _():
        kv_copy(me).start()

    key_scale = dk ** (-0.5)
    position = lax.broadcasted_iota(jnp.int32, (rows, 1), 0).astype(jnp.float32)
    rq, rk, rv = [], [], []
    for h in range(hr):
        rq.append(proj_buf[:, h * dk : (h + 1) * dk])
        rk.append(proj_buf[:, (hr + h) * dk : (hr + h + 1) * dk])
        rv.append(proj_buf[:, 2 * hr * dk + h * vd : 2 * hr * dk + (h + 1) * vd])
        keys = rk[h].astype(jnp.float32) * key_scale
        trailing = jnp.exp((rows - 1.0 - position) * decay_ref[h])
        sum_buf[me, h] = lax.dot_general(
            keys * trailing, rv[h].astype(jnp.float32), TN, precision=highest, preferred_element_type=jnp.float32
        )

    @pl.when(has_up)
    def _():
        sum_copy(me).start()

    row_id = lax.broadcasted_iota(jnp.int32, (rows, rows), 0)
    col_id = lax.broadcasted_iota(jnp.int32, (rows, rows), 1)
    causal = col_id <= row_id
    fq = [proj_buf[:, hr * (2 * dk + vd) + h * fd : hr * (2 * dk + vd) + (h + 1) * fd] for h in range(fh)]
    own_rows = pl.ds(pl.multiple_of(me * rows, rows), rows)
    own_gates = gates_ref[own_rows, :]

    def attend(src, current, diagonal):
        key_cols = pl.ds(pl.multiple_of(src * rows, rows), rows)
        following = []
        for h in range(fh):
            top, total, weighted = current[h]
            k = kv_buf[src, :, h * fd : (h + 1) * fd]
            v = kv_buf[src, :, (fh + h) * fd : (fh + h + 1) * fd]
            logits = lax.dot_general(fq[h], k, NT, preferred_element_type=jnp.float32) * fd ** (-0.5)
            logits = logits + own_gates[:, h : h + 1] - gates_t_ref[h : h + 1, key_cols]
            if diagonal:
                logits = jnp.where(causal, logits, -jnp.inf)
            top_new = jnp.maximum(top, jnp.max(logits, axis=-1, keepdims=True))
            p = jnp.exp(logits - top_new)
            rescale = jnp.exp(top - top_new)
            total = total * rescale + jnp.sum(p, axis=-1, keepdims=True)
            weighted = weighted * rescale + jnp.dot(p.astype(jnp.bfloat16), v, preferred_element_type=jnp.float32)
            following.append((top_new, total, weighted))
        return tuple(following)

    start = tuple(
        (
            jnp.full((rows, 1), -1e30, jnp.float32),
            jnp.zeros((rows, 1), jnp.float32),
            jnp.zeros((rows, fd), jnp.float32),
        )
        for _ in range(fh)
    )
    current = attend(me, start, True)

    inner = []
    distance = jnp.maximum(row_id - col_id, 0).astype(jnp.float32)
    for h in range(hr):
        scores = lax.dot_general(rq[h], rk[h], NT, preferred_element_type=jnp.float32) * key_scale
        scores = jnp.where(causal, scores * jnp.exp(distance * decay_ref[h]), 0.0)
        inner.append(
            jnp.dot(scores, rv[h].astype(jnp.float32), precision=highest, preferred_element_type=jnp.float32)
        )

    offset = (me * rows).astype(jnp.float32)
    lone = jnp.zeros((dk, vd), jnp.float32)
    entering = tuple(jnp.exp(lone + offset * decay_ref[h]) * state_ref[h] for h in range(hr))

    def earlier(k, carry):
        current, entering = carry
        src = me - k
        kv_copy(src).wait_recv()

        @pl.when(has_up)
        def _():
            kv_copy(src).start()

        sum_copy(src).wait_recv()

        @pl.when(has_up)
        def _():
            sum_copy(src).start()

        gap = ((k - 1) * rows).astype(jnp.float32)
        entering = tuple(
            entering[h] + jnp.exp(lone + gap * decay_ref[h]) * sum_buf[src, h] for h in range(hr)
        )
        return attend(src, current, False), entering

    current, entering = lax.fori_loop(1, me + 1, earlier, (current, entering))

    for h in range(hr):
        leading = jnp.exp((position + 1.0) * decay_ref[h])
        carried = jnp.dot(
            rq[h].astype(jnp.float32), entering[h], precision=highest, preferred_element_type=jnp.float32
        )
        raw = inner[h] + carried * leading
        center = raw - jnp.mean(raw, axis=-1, keepdims=True)
        variance = jnp.mean(center * center, axis=-1, keepdims=True)
        cols = slice(h * vd, (h + 1) * vd)
        mix_buf[:, cols] = (center * lax.rsqrt(variance + epsilon) * hgain_ref[:, cols]).astype(jnp.bfloat16)
    for h in range(fh):
        top, total, weighted = current[h]
        cols = slice(hr * vd + h * fd, hr * vd + (h + 1) * fd)
        mix_buf[:, cols] = (weighted / total).astype(jnp.bfloat16)

    outs.arrive()
    block = rows // n_tp

    def rs_copy(d):
        return rdma(
            rs_send.at[d - 1], rs_buf.at[d - 1], rs_s.at[d - 1], rs_r.at[d - 1], tp=lax.rem(t + d, n_tp)
        )

    def partial(owner):
        mine = mix_buf[pl.ds(pl.multiple_of(owner * block, block), block), :]
        return lax.dot_general(mine, wout_buf[...], NT, preferred_element_type=jnp.float32).astype(jnp.bfloat16)

    for d in reversed(range(1, n_tp)):
        rs_send[d - 1] = partial(lax.rem(t + d, n_tp))
        rs_copy(d).start()
    summed = partial(t).astype(jnp.float32)
    for d in range(1, n_tp):
        rs_copy(d).wait_recv()
        summed = summed + rs_buf[d - 1].astype(jnp.float32)
    out_ref[...] = summed.astype(jnp.bfloat16)

    for d in range(1, n_tp):
        tok_copy(d).wait_send()
        rs_copy(d).wait_send()
    weights.finish()
    outs.finish()

    @pl.when(has_up)
    def _():
        def step(src, _):
            kv_copy(src).wait_send()
            sum_copy(src).wait_send()
            return 0

        lax.fori_loop(0, me + 1, step, 0)


def local(
    n,
    n_tp,
    n_grp,
    tokens,
    norm_gain,
    ret_query_weight,
    ret_key_weight,
    ret_value_weight,
    fox_query_weight,
    fox_key_weight,
    fox_value_weight,
    ret_decay,
    ret_state,
    head_norm_gain,
    fox_gates,
    ret_out_weight,
    fox_out_weight,
):
    rows, feats = tokens.shape
    hr, dk, vd = ret_state.shape
    fh = fox_gates.shape[1]
    fd = fox_query_weight.shape[1] // fh
    joined = jnp.concatenate(
        (
            ret_query_weight,
            ret_key_weight,
            ret_value_weight,
            fox_query_weight,
            fox_key_weight,
            fox_value_weight,
        ),
        axis=1,
    )
    out_joined = jnp.concatenate((ret_out_weight, fox_out_weight), axis=0).T
    width, depth = joined.shape[1], out_joined.shape[1]
    columns = out_joined.shape[0] * n

    def chunks_of(count):
        part = count // n_grp
        return 2 if part % 32 == 0 else 1

    chunks, out_chunks = chunks_of(joined.shape[0]), chunks_of(out_joined.shape[0])
    dma = pltpu.SemaphoreType.DMA

    def gather_sems(parts):
        return [
            dma((n * parts,)),
            dma((n * parts,)),
            dma((n * parts,)),
            dma((max(n_grp - 1, 1) * n * parts,)),
            dma((max(n_grp - 1, 1) * n * parts,)),
            dma,
        ]

    vmem = pl.BlockSpec(memory_space=pltpu.VMEM)
    smem = pl.BlockSpec(memory_space=pltpu.SMEM)
    size = (n, n_tp, n_grp, hr, dk, vd, fh, fd, chunks, out_chunks)
    block = rows // n_tp
    peers = max(n_tp - 1, 1)
    return pl.pallas_call(
        functools.partial(kernel, size),
        out_shape=jax.ShapeDtypeStruct((block, columns), jnp.bfloat16),
        in_specs=[vmem, vmem, vmem, smem, vmem, vmem, vmem, vmem, vmem],
        out_specs=vmem,
        scratch_shapes=[
            pltpu.VMEM((n_tp, rows, feats), jnp.bfloat16),
            pltpu.VMEM((n * joined.shape[0], width), jnp.bfloat16),
            pltpu.VMEM((columns, depth), jnp.bfloat16),
            pltpu.VMEM((rows, n_tp * feats), jnp.bfloat16),
            pltpu.VMEM((rows, width), jnp.bfloat16),
            pltpu.VMEM((n, rows, 2 * fh * fd), jnp.bfloat16),
            pltpu.VMEM((n, hr, dk, vd), jnp.float32),
            pltpu.VMEM((rows, depth), jnp.bfloat16),
            pltpu.VMEM((peers, block, columns), jnp.bfloat16),
            pltpu.VMEM((peers, block, columns), jnp.bfloat16),
            dma((peers,)),
            dma((peers,)),
            dma,
            dma((n,)),
            dma((n,)),
            dma((n,)),
            dma((n,)),
            dma((peers,)),
            dma((peers,)),
        ]
        + gather_sems(chunks)
        + gather_sems(out_chunks),
        compiler_params=pltpu.CompilerParams(
            collective_id=0, has_side_effects=True, vmem_limit_bytes=48 * 1024 * 1024
        ),
        name="layer",
    )(
        tokens,
        norm_gain[None, :],
        joined,
        ret_decay,
        ret_state,
        head_norm_gain[None, :],
        fox_gates,
        fox_gates.T,
        out_joined,
    )


def solution(mesh):
    placed = (
        P(("grp", "sp"), "tp"),
        P(),
        P("sp", "tp"),
        P("sp", "tp"),
        P("sp", "tp"),
        P("sp", "tp"),
        P("sp", "tp"),
        P("sp", "tp"),
        P("tp"),
        P(("grp", "tp"), None, None),
        P("tp"),
        P("grp", "tp"),
        P("tp", "sp"),
        P("tp", "sp"),
    )
    body = functools.partial(local, mesh.shape["sp"], mesh.shape["tp"], mesh.shape["grp"])
    return jax.shard_map(
        body, mesh=mesh, in_specs=placed, out_specs=P(("grp", "sp", "tp"), None), check_vma=False
    )
```

time: 228 us -> 68.3 us (0.30)
  blocking collectives: 166 us -> 0 us
  Pallas kernels: 0 us -> 61.6 us
  waiting for transfers between devices: 26.6 us -> 0 us
  between operations: 13.7 us -> 0.13 us
  matrix products: 10.1 us -> 0 us
  other arithmetic: 5.95 us -> 0.03 us
  local copies, waits for them, and re-layouts: 3.75 us -> 6.26 us
    all_gather x11 -> x0, blocking collectives: 166 us -> none  [the longest x1 16.2 us: local(): lax.all_gather(fox_key_weight, 'sp', axis=0, tiled=True)]
    pallas_call x0 -> x1, Pallas kernels: none -> 61.6 us  [local(): pl.pallas_call(functools.partial(kernel, size), out_shape=jax.ShapeDtypeS...]
    reduce_scatter x1 -> x0, waiting for transfers between devices: 25.9 us -> none  [local(): lax.psum_scatter((jnp.dot(retention_mixed, ret_full, preferred_element_ty...]
    dot_general x15 -> x0, matrix products: 10.1 us -> none  [the longest x6 5.1 us: local(): jnp.dot(normed, portion, preferred_element_type=jnp.float32)]
    unnamed x30 -> x32, local copies, waits for them, and re-layouts: 0.07 us -> 5.95 us
  transfers between devices with their start and end apart: 2 -> 0, of which waited for: 1 -> 0; matrix products, arithmetic and copies ran while one was open for 3% -> 0% of each run, Pallas kernels for 0% -> 0%
where the time goes in v1:
time: 68.3 us; the launch traced here: 68.1 us
  Pallas kernels  61.6 us (90%)
  local copies, waits for them, and re-layouts  6.26 us (9%)
    pallas_call x1, Pallas kernels, local(): pl.pallas_call(functools.partial(kernel, size), out_shape=jax.ShapeDtypeS...  61.6 us
    unnamed x32, local copies, waits for them, and re-layouts  5.95 us

profile of v1, /device:TPU:24, one launch (start us, length us, event | category | flops | bytes accessed | tf_op | source)
XLA Modules:
  0.0 68.1 jit_solution(13984973235176038178)
XLA Ops:
  0.0 0.0 copy-start.12
  0.0 1.0 %copy.15 = bf16[512,64]{1,0:T(8,128)(2,1)S(1)} copy(bf16[512,64]{0,1:T(8,128)(2,1)} %param.16) | data formatting | bytes 131072 | tf_op args[2]
  1.0 0.0 copy-done.12
  1.0 0.0 copy-start.6
  1.0 0.1 copy.16
  1.1 0.8 %copy-done.6 = bf16[128,512]{1,0:T(8,128)(2,1)S(1)} copy-done((bf16[128,512]{1,0:T(8,128)(2,1)S(1)}, bf16[128,512]{1,0:T(8,128)(2,1)}, u32[]{:S(2)}) %copy-start.6) | copy-done | bytes 131096
  1.9 0.0 copy-start.7
  1.9 0.1 copy.17
  2.0 0.8 %copy-done.7 = bf16[128,512]{1,0:T(8,128)(2,1)S(1)} copy-done((bf16[128,512]{1,0:T(8,128)(2,1)S(1)}, bf16[128,512]{1,0:T(8,128)(2,1)}, u32[]{:S(2)}) %copy-start.7) | copy-done | bytes 131096
  2.8 0.1 copy.18
  2.9 0.0 copy-start.8
  3.0 0.0 copy-start.9
  3.0 0.0 copy-start.10
  3.0 0.0 copy-start.11
  3.0 0.8 %copy-done.8 = bf16[512,128]{1,0:T(8,128)(2,1)S(1)} copy-done((bf16[512,128]{1,0:T(8,128)(2,1)S(1)}, bf16[512,128]{1,0:T(8,128)(2,1)}, u32[]{:S(2)}) %copy-start.8) | copy-done | bytes 131096
  3.9 0.1 copy-done.9
  3.9 0.1 copy-done.10
  4.0 0.1 copy-done.11
  4.0 0.0 copy-start.2
  4.0 0.3 concatenate.6.w_ref
  4.4 0.4 copy-done.2
  4.7 0.0 copy-start
  4.7 0.0 copy-start.1
  4.7 0.0 copy-start.3
  4.8 0.0 copy-start.4
  4.8 0.0 copy-start.5
  4.8 0.2 copy.19.gates_ref
  5.0 0.7 %copy-done = bf16[256,512]{1,0:T(8,128)(2,1)S(1)} copy-done((bf16[256,512]{1,0:T(8,128)(2,1)S(1)}, bf16[256,512]{1,0:T(8,128)(2,1)}, u32[]{:S(2)}) %copy-start) | copy-done | bytes 262168
  5.7 0.0 copy-done.1
  5.7 0.0 copy-done.3
  5.7 0.0 copy-done.4
  5.7 0.0 copy-done.5
  5.7 61.6 %layer.1 = bf16[64,2048]{1,0:T(8,128)(2,1)S(1)} custom-call(bf16[256,512]{1,0:T(8,128)(2,1)S(1)} %copy-done, f32[1,2048]{1,0:T(1,128)S(1)} %bitcast.6, bf16[512,640]{1,0:T(8,128)(2,1)S(1)} %concatenate.6.w_ref, f32[2]{0:T(128)S(1)} %copy-done.4, f32[2,32,64]{2,1,0:T(8,128)S(1)} %copy-done.1, f32[1,128]{1,0:T(1,128)S(1)} %bitcast.7, ...), custom_call_target="tpu_custom_call" | custom-call | tf_op jit(solution)/shard_map/layer/pallas_call | solution.py:448
  67.3 0.7 %copy.21 = bf16[64,2048]{1,0:T(8,128)(2,1)} copy(bf16[64,2048]{1,0:T(8,128)(2,1)S(1)} %layer.1) | data formatting | bytes 524288
  (1 shorter events, 0.0 us)
Async XLA Ops:
  0.0 1.0 %copy-start.12 = (bf16[512,64]{0,1:T(8,128)(2,1)S(1)}, bf16[512,64]{0,1:T(8,128)(2,1)}, u32[]{:S(2)}) copy-start(bf16[512,64]{0,1:T(8,128)(2,1)} %param.17) | copy-start | bytes 196612
  1.0 0.9 %copy-start.6 = (bf16[128,512]{1,0:T(8,128)(2,1)S(1)}, bf16[128,512]{1,0:T(8,128)(2,1)}, u32[]{:S(2)}) copy-start(bf16[128,512]{1,0:T(8,128)(2,1)} %param.26) | copy-start | bytes 393220
  1.9 0.9 %copy-start.7 = (bf16[128,512]{1,0:T(8,128)(2,1)S(1)}, bf16[128,512]{1,0:T(8,128)(2,1)}, u32[]{:S(2)}) copy-start(bf16[128,512]{1,0:T(8,128)(2,1)} %param.27) | copy-start | bytes 393220
  2.9 0.9 %copy-start.8 = (bf16[512,128]{1,0:T(8,128)(2,1)S(1)}, bf16[512,128]{1,0:T(8,128)(2,1)}, u32[]{:S(2)}) copy-start(bf16[512,128]{1,0:T(8,128)(2,1)} %param.18) | copy-start | bytes 393220
  3.0 1.0 %copy-start.9 = (bf16[512,128]{1,0:T(8,128)(2,1)S(1)}, bf16[512,128]{1,0:T(8,128)(2,1)}, u32[]{:S(2)}) copy-start(bf16[512,128]{1,0:T(8,128)(2,1)} %param.19) | copy-start | bytes 393220
  3.0 1.0 %copy-start.10 = (bf16[512,128]{1,0:T(8,128)(2,1)S(1)}, bf16[512,128]{1,0:T(8,128)(2,1)}, u32[]{:S(2)}) copy-start(bf16[512,128]{1,0:T(8,128)(2,1)} %param.20) | copy-start | bytes 393220
  3.0 1.1 %copy-start.11 = (bf16[512,128]{1,0:T(8,128)(2,1)S(1)}, bf16[512,128]{1,0:T(8,128)(2,1)}, u32[]{:S(2)}) copy-start(bf16[512,128]{1,0:T(8,128)(2,1)} %param.21) | copy-start | bytes 393220
  4.0 0.7 %copy-start.2 = (f32[1024,2]{0,1:T(2,128)S(1)}, f32[1024,2]{0,1:T(2,128)}, u32[]{:S(2)}) copy-start(f32[1024,2]{0,1:T(2,128)} %param.25) | copy-start | bytes 24580
  4.7 0.9 %copy-start = (bf16[256,512]{1,0:T(8,128)(2,1)S(1)}, bf16[256,512]{1,0:T(8,128)(2,1)}, u32[]{:S(2)}) copy-start(bf16[256,512]{1,0:T(8,128)(2,1)} %tok_ref.1) | copy-start | bytes 786436
  4.7 1.0 %copy-start.1 = (f32[2,32,64]{2,1,0:T(8,128)S(1)}, f32[2,32,64]{2,1,0:T(8,128)}, u32[]{:S(2)}) copy-start(f32[2,32,64]{2,1,0:T(8,128)} %state_ref.1) | copy-start | bytes 49156
  4.7 1.0 %copy-start.3 = (f32[2048]{0:T(1024)S(1)}, f32[2048]{0:T(1024)}, u32[]{:S(2)}) copy-start(f32[2048]{0:T(1024)} %param.15) | copy-start | bytes 24580
  4.8 1.0 %copy-start.4 = (f32[2]{0:T(128)S(1)}, f32[2]{0:T(128)}, u32[]{:S(2)}) copy-start(f32[2]{0:T(128)} %decay_ref.1) | copy-start | bytes 28
  4.8 0.9 %copy-start.5 = (f32[128]{0:T(128)S(1)}, f32[128]{0:T(128)}, u32[]{:S(2)}) copy-start(f32[128]{0:T(128)} %param.24) | copy-start | bytes 1540

commit v2 on v1

v2 whole, which is shorter than its diff:
```python
import functools

import jax
import jax.numpy as jnp
from jax import lax
from jax.experimental import pallas as pl
from jax.experimental.pallas import tpu as pltpu
from jax.sharding import PartitionSpec as P

epsilon = 1e-06
highest = lax.Precision.HIGHEST
NT = (((1,), (1,)), ((), ()))
TN = (((0,), (0,)), ((), ()))


def rdma(src, dst, send_sem, recv_sem, **target):
    return pltpu.make_async_remote_copy(
        src_ref=src,
        dst_ref=dst,
        send_sem=send_sem,
        recv_sem=recv_sem,
        device_id=target,
        device_id_type=pl.DeviceIdType.MESH,
    )


class LineGather:
    def __init__(self, owns, place, sems, n, n_grp, me, g):
        self.owns, self.place, self.n, self.n_grp, self.me, self.g = owns, place, n, n_grp, me, g
        self.up, self.down, self.zr, self.ys, self.yr, self.loc = sems
        self.arrays = len(owns)
        self.rows = owns[0].shape[0]
        self.step = self.rows // n_grp

    def piece(self, part, src, c):
        return self.place(src, c, part * self.step, self.step)

    def own_piece(self, c):
        return self.owns[c].at[pl.ds(pl.multiple_of(self.g * self.step, self.step), self.step)]

    def hop(self, sems, to, src, c, first=False):
        here = self.own_piece(c) if first else self.piece(self.g, src, c)
        at = src * self.arrays + c
        return rdma(here, self.piece(self.g, src, c), sems.at[at], self.zr.at[at], sp=to)

    def side(self, d, src, c):
        at = ((d - 1) * self.n + src) * self.arrays + c
        here = self.piece(self.g, src, c)
        return rdma(here, here, self.ys.at[at], self.yr.at[at], grp=lax.rem(self.g + d, self.n_grp))

    def side_in(self, d, src, c):
        at = ((d - 1) * self.n + src) * self.arrays + c
        part = lax.rem(self.g + self.n_grp - d, self.n_grp)
        here = self.piece(part, src, c)
        return rdma(here, here, self.ys.at[at], self.yr.at[at], grp=part)

    def local(self, c):
        return pltpu.make_async_copy(self.owns[c], self.place(self.me, c, 0, self.rows), self.loc.at[c])

    def start(self):
        me, n = self.me, self.n
        for c in range(self.arrays):

            @pl.when(me + 1 < n)
            def _():
                self.hop(self.up, me + 1, me, c, True).start()

            @pl.when(me >= 1)
            def _():
                self.hop(self.down, me - 1, me, c, True).start()

        for c in range(self.arrays):
            self.local(c).start()

    def relay(self, k):
        me, n = self.me, self.n
        for c in range(self.arrays):
            for src, sems, to in ((me - k, self.up, me + 1), (me + k, self.down, me - 1)):

                @pl.when((src >= 0) & (src < n))
                def _(src=src, sems=sems, to=to):
                    self.hop(sems, me, src, c).wait_recv()

                    @pl.when((to >= 0) & (to < n))
                    def _():
                        self.hop(sems, to, src, c).start()

                    for d in range(1, self.n_grp):
                        self.side(d, src, c).start()

    def arrive_shard(self, src, arrays):
        for c in arrays:
            for d in range(1, self.n_grp):
                self.side_in(d, src, c).wait_recv()

    def arrive(self, arrays):
        for c in arrays:
            self.local(c).wait()

        def step(k, _):
            self.arrive_shard(lax.rem(self.me + k, self.n), arrays)
            return 0

        lax.fori_loop(1, self.n, step, 0)

    def finish(self):
        me, n = self.me, self.n

        def step(src, _):
            for c in range(self.arrays):

                @pl.when((src <= me) & (me + 1 < n))
                def _():
                    self.hop(self.up, me, src, c).wait_send()

                @pl.when((src >= me) & (me >= 1))
                def _():
                    self.hop(self.down, me, src, c).wait_send()

                @pl.when(src != me)
                def _():
                    for d in range(1, self.n_grp):
                        self.side(d, src, c).wait_send()

            return 0

        lax.fori_loop(0, n, step, 0)


def kernel(
    size,
    tok_ref,
    gain_ref,
    wq_ref,
    wk_ref,
    wrv_ref,
    wfq_ref,
    wfk_ref,
    wfv_ref,
    decay_ref,
    state_ref,
    hgain_ref,
    gates_ref,
    ret_out_ref,
    fox_out_ref,
    out_ref,
    tok_buf,
    qk_own,
    w_buf,
    wout_buf,
    norm_buf,
    proj_buf,
    kv_buf,
    sum_buf,
    mix_buf,
    rs_send,
    rs_buf,
    top_buf,
    total_buf,
    weighted_buf,
    tok_s,
    tok_r,
    tok_loc,
    kv_s,
    kv_r,
    sum_s,
    sum_r,
    rs_s,
    rs_r,
    *gather_sems,
):
    n, n_tp, n_grp, hr, dk, vd, fh, fd, direct = size
    me, t, g = lax.axis_index("sp"), lax.axis_index("tp"), lax.axis_index("grp")
    rows, feats = tok_ref.shape
    owns = [wfk_ref, wfv_ref, wfq_ref, wrv_ref, qk_own]
    starts = [0]
    for own in owns:
        starts.append(starts[-1] + own.shape[1])
    shard = qk_own.shape[0]

    def weight_place(src, c, first, count):
        start = pl.multiple_of(src * shard + first, count)
        return w_buf.at[pl.ds(start, count), starts[c] : starts[c + 1]]

    depth = mix_buf.shape[1] // 2
    out_cols = ret_out_ref.shape[1] if direct else ret_out_ref.shape[0]

    def out_place(src, c, first, count):
        if direct:
            start = pl.multiple_of(c * depth + first, count)
            return wout_buf.at[pl.ds(start, count), pl.ds(pl.multiple_of(src * out_cols, out_cols), out_cols)]
        start = pl.multiple_of(src * out_cols + first, count)
        return wout_buf.at[pl.ds(start, count), c * depth : (c + 1) * depth]

    weights = LineGather(owns, weight_place, gather_sems[:6], n, n_grp, me, g)
    outs = LineGather([ret_out_ref, fox_out_ref], out_place, gather_sems[6:], n, n_grp, me, g)

    barrier = pltpu.get_barrier_semaphore()

    def greet(**target):
        pl.semaphore_signal(barrier, inc=1, device_id=target, device_id_type=pl.DeviceIdType.MESH)

    has_up, has_down = me + 1 < n, me >= 1
    for d in range(1, n_tp):
        greet(tp=lax.rem(t + d, n_tp))
    for d in range(1, n_grp):
        greet(grp=lax.rem(g + d, n_grp))

    @pl.when(has_up)
    def _():
        greet(sp=me + 1)

    @pl.when(has_down)
    def _():
        greet(sp=me - 1)

    turned = jnp.concatenate((wq_ref[...], wk_ref[...]), axis=0).astype(jnp.float32)
    qk_own[...] = turned.T.astype(jnp.bfloat16)

    count = n_tp - 1 + n_grp - 1 + has_up.astype(jnp.int32) + has_down.astype(jnp.int32)
    pl.semaphore_wait(barrier, count)

    def tok_copy(d):
        return rdma(tok_ref, tok_buf.at[t], tok_s.at[d - 1], tok_r.at[d - 1], tp=lax.rem(t + d, n_tp))

    def tok_in(d):
        src = lax.rem(t + n_tp - d, n_tp)
        return rdma(tok_ref, tok_buf.at[src], tok_s.at[d - 1], tok_r.at[d - 1], tp=src)

    weights.start()
    tok_local = pltpu.make_async_copy(tok_ref, tok_buf.at[t], tok_loc)
    for d in range(1, n_tp):
        tok_copy(d).start()
    tok_local.start()

    def weight_step(k, _):
        weights.relay(k)
        return 0

    lax.fori_loop(1, n, weight_step, 0)
    outs.start()

    tok_local.wait()
    for d in range(1, n_tp):
        tok_in(d).wait_recv()
    squares = jnp.zeros((rows, 1), jnp.float32)
    for i in range(n_tp):
        part = tok_buf[i].astype(jnp.float32)
        squares = squares + jnp.sum(part * part, axis=-1, keepdims=True)
    scale = lax.rsqrt(squares * (1.0 / (n_tp * feats)) + epsilon)
    for i in range(n_tp):
        part = tok_buf[i].astype(jnp.float32)
        cols = slice(i * feats, (i + 1) * feats)
        norm_buf[:, cols] = (part * scale * gain_ref[:, cols]).astype(jnp.bfloat16)

    def kv_copy(src):
        return rdma(kv_buf.at[src], kv_buf.at[src], kv_s.at[src], kv_r.at[src], sp=jnp.minimum(me + 1, n - 1))

    def sum_copy(src):
        return rdma(sum_buf.at[src], sum_buf.at[src], sum_s.at[src], sum_r.at[src], sp=jnp.minimum(me + 1, n - 1))

    weights.arrive((0, 1))
    kv_buf[me] = jnp.dot(
        norm_buf[...], w_buf[:, : starts[2]], preferred_element_type=jnp.float32
    ).astype(jnp.bfloat16)

    @pl.when(has_up)
    def _():
        kv_copy(me).start()

    if n > 1:
        outs.relay(1)
    weights.arrive((2, 3, 4))
    proj_buf[...] = jnp.dot(
        norm_buf[...], w_buf[:, starts[2] :], preferred_element_type=jnp.float32
    ).astype(jnp.bfloat16)
    rv_at, rq_at = starts[3] - starts[2], starts[4] - starts[2]

    key_scale = dk ** (-0.5)
    position = lax.broadcasted_iota(jnp.int32, (rows, 1), 0).astype(jnp.float32)
    rq, rk, rv = [], [], []
    for h in range(hr):
        rq.append(proj_buf[:, rq_at + h * dk : rq_at + (h + 1) * dk])
        rk.append(proj_buf[:, rq_at + (hr + h) * dk : rq_at + (hr + h + 1) * dk])
        rv.append(proj_buf[:, rv_at + h * vd : rv_at + (h + 1) * vd])
        keys = rk[h].astype(jnp.float32) * key_scale
        trailing = jnp.exp((rows - 1.0 - position) * decay_ref[h])
        sum_buf[me, h] = lax.dot_general(
            keys * trailing, rv[h].astype(jnp.float32), TN, precision=highest, preferred_element_type=jnp.float32
        )

    @pl.when(has_up)
    def _():
        sum_copy(me).start()

    row_id = lax.broadcasted_iota(jnp.int32, (rows, rows), 0)
    col_id = lax.broadcasted_iota(jnp.int32, (rows, rows), 1)
    causal = col_id <= row_id
    own_cols = pl.ds(pl.multiple_of(me * rows, rows), rows)
    own_gates = [
        jnp.sum(jnp.where(row_id == col_id, gates_ref[h : h + 1, own_cols], 0.0), axis=1, keepdims=True)
        for h in range(fh)
    ]

    def attend(src, diagonal):
        key_cols = pl.ds(pl.multiple_of(src * rows, rows), rows)
        for h in range(fh):
            query = proj_buf[:, h * fd : (h + 1) * fd]
            k = kv_buf[src, :, h * fd : (h + 1) * fd]
            v = kv_buf[src, :, (fh + h) * fd : (fh + h + 1) * fd]
            logits = lax.dot_general(query, k, NT, preferred_element_type=jnp.float32) * fd ** (-0.5)
            logits = logits + own_gates[h] - gates_ref[h : h + 1, key_cols]
            if diagonal:
                logits = jnp.where(causal, logits, -jnp.inf)
            top_new = jnp.max(logits, axis=-1, keepdims=True)
            if not diagonal:
                top = top_buf[h]
                top_new = jnp.maximum(top, top_new)
            p = jnp.exp(logits - top_new)
            total = jnp.sum(p, axis=-1, keepdims=True)
            weighted = jnp.dot(p.astype(jnp.bfloat16), v, preferred_element_type=jnp.float32)
            if not diagonal:
                rescale = jnp.exp(top - top_new)
                total = total_buf[h] * rescale + total
                weighted = weighted_buf[h] * rescale + weighted
            top_buf[h] = top_new
            total_buf[h] = total
            weighted_buf[h] = weighted

    def forward(k):
        src = me - k

        @pl.when(src >= 0)
        def _():
            kv_copy(src).wait_recv()

            @pl.when(has_up)
            def _():
                kv_copy(src).start()

            sum_copy(src).wait_recv()

            @pl.when(has_up)
            def _():
                sum_copy(src).start()

    attend(me, True)

    offset = (me * rows).astype(jnp.float32)
    lone = jnp.zeros((dk, vd), jnp.float32)

    def step(k, entering):
        src = me - k
        forward(k)

        @pl.when(k + 1 < n)
        def _():
            outs.relay(k + 1)

        @pl.when(src >= 0)
        def _():
            attend(src, False)

        gap = ((k - 1) * rows).astype(jnp.float32)
        there = jnp.maximum(src, 0)
        return tuple(
            entering[h]
            + jnp.where(src >= 0, jnp.exp(lone + gap * decay_ref[h]) * sum_buf[there, h], 0.0)
            for h in range(hr)
        )

    entering = tuple(jnp.exp(lone + offset * decay_ref[h]) * state_ref[h] for h in range(hr))
    entering = lax.fori_loop(1, n, step, entering)

    distance = jnp.maximum(row_id - col_id, 0).astype(jnp.float32)
    for h in range(hr):
        scores = lax.dot_general(rq[h], rk[h], NT, preferred_element_type=jnp.float32) * key_scale
        scores = jnp.where(causal, scores * jnp.exp(distance * decay_ref[h]), 0.0)
        inner = jnp.dot(scores, rv[h].astype(jnp.float32), precision=highest, preferred_element_type=jnp.float32)
        leading = jnp.exp((position + 1.0) * decay_ref[h])
        carried = jnp.dot(
            rq[h].astype(jnp.float32), entering[h], precision=highest, preferred_element_type=jnp.float32
        )
        raw = inner + carried * leading
        center = raw - jnp.mean(raw, axis=-1, keepdims=True)
        variance = jnp.mean(center * center, axis=-1, keepdims=True)
        cols = slice(h * vd, (h + 1) * vd)
        mix_buf[:, cols] = (center * lax.rsqrt(variance + epsilon) * hgain_ref[:, cols]).astype(jnp.bfloat16)
    for h in range(fh):
        cols = slice(hr * vd + h * fd, hr * vd + (h + 1) * fd)
        mix_buf[:, cols] = (weighted_buf[h] / total_buf[h]).astype(jnp.bfloat16)

    block = rows // n_tp
    columns = rs_send.shape[1]
    wide = out_cols if direct else columns
    pieces = columns // wide
    mine = pl.ds(pl.multiple_of(t * block, block), block)

    def rs_copy(d, piece):
        to = lax.rem(t + d, n_tp)
        cols = pl.ds(pl.multiple_of(piece * wide, wide), wide)
        at = (d - 1) * pieces + piece
        return rdma(
            rs_send.at[pl.ds(pl.multiple_of(to * block, block), block), cols],
            rs_buf.at[d - 1, :, cols],
            rs_s.at[at],
            rs_r.at[at],
            tp=to,
        )

    def project(piece):
        cols = pl.ds(pl.multiple_of(piece * wide, wide), wide)
        if direct:
            value = jnp.dot(mix_buf[...], wout_buf[:, cols], preferred_element_type=jnp.float32)
        else:
            value = lax.dot_general(mix_buf[...], wout_buf[...], NT, preferred_element_type=jnp.float32)
        rs_send[:, cols] = value.astype(jnp.bfloat16)
        for d in range(1, n_tp):
            rs_copy(d, piece).start()

    if direct:
        for c in range(2):
            outs.local(c).wait()
        project(me)

        def out_step(k, _):
            for src in (me - k, me + k):

                @pl.when((src >= 0) & (src < n))
                def _(src=src):
                    outs.arrive_shard(src, (0, 1))
                    project(src)

            return 0

        lax.fori_loop(1, n, out_step, 0)
    else:
        outs.arrive((0, 1))
        project(0)

    summed = rs_send[mine, :].astype(jnp.float32)
    for d in range(1, n_tp):
        for piece in range(pieces):
            rs_copy(d, piece).wait_recv()
        summed = summed + rs_buf[d - 1].astype(jnp.float32)
    out_ref[...] = summed.astype(jnp.bfloat16)

    for d in range(1, n_tp):
        tok_copy(d).wait_send()
        for piece in range(pieces):
            rs_copy(d, piece).wait_send()
    weights.finish()
    outs.finish()

    @pl.when(has_up)
    def _():
        def step(src, _):
            kv_copy(src).wait_send()
            sum_copy(src).wait_send()
            return 0

        lax.fori_loop(0, me + 1, step, 0)


def local(
    n,
    n_tp,
    n_grp,
    tokens,
    norm_gain,
    ret_query_weight,
    ret_key_weight,
    ret_value_weight,
    fox_query_weight,
    fox_key_weight,
    fox_value_weight,
    ret_decay,
    ret_state,
    head_norm_gain,
    fox_gates,
    ret_out_weight,
    fox_out_weight,
):
    rows, feats = tokens.shape
    hr, dk, vd = ret_state.shape
    fh = fox_gates.shape[1]
    fd = fox_query_weight.shape[1] // fh
    shard = ret_query_weight.shape[0]
    width = 2 * hr * dk + hr * vd + 3 * fh * fd
    depth, out_cols = ret_out_weight.shape
    columns = out_cols * n
    direct = out_cols % 128 == 0
    if not direct:
        ret_out_weight, fox_out_weight = ret_out_weight.T, fox_out_weight.T
    dma = pltpu.SemaphoreType.DMA

    def gather_sems(arrays):
        side = max(n_grp - 1, 1) * n * arrays
        return [
            dma((n * arrays,)),
            dma((n * arrays,)),
            dma((n * arrays,)),
            dma((side,)),
            dma((side,)),
            dma((arrays,)),
        ]

    vmem = pl.BlockSpec(memory_space=pltpu.VMEM)
    smem = pl.BlockSpec(memory_space=pltpu.SMEM)
    hbm = pl.BlockSpec(memory_space=pl.ANY)
    size = (n, n_tp, n_grp, hr, dk, vd, fh, fd, direct)
    block = rows // n_tp
    peers = max(n_tp - 1, 1)
    pieces = n if direct else 1
    return pl.pallas_call(
        functools.partial(kernel, size),
        out_shape=jax.ShapeDtypeStruct((block, columns), jnp.bfloat16),
        in_specs=[hbm, vmem, vmem, vmem, hbm, hbm, hbm, hbm, smem, vmem, vmem, vmem, hbm, hbm],
        out_specs=vmem,
        scratch_shapes=[
            pltpu.VMEM((n_tp, rows, feats), jnp.bfloat16),
            pltpu.VMEM((shard, 2 * hr * dk), jnp.bfloat16),
            pltpu.VMEM((n * shard, width), jnp.bfloat16),
            pltpu.VMEM((2 * depth, columns) if direct else (columns, 2 * depth), jnp.bfloat16),
            pltpu.VMEM((rows, n_tp * feats), jnp.bfloat16),
            pltpu.VMEM((rows, width - 2 * fh * fd), jnp.bfloat16),
            pltpu.VMEM((n, rows, 2 * fh * fd), jnp.bfloat16),
            pltpu.VMEM((n, hr, dk, vd), jnp.float32),
            pltpu.VMEM((rows, 2 * depth), jnp.bfloat16),
            pltpu.VMEM((rows, columns), jnp.bfloat16),
            pltpu.VMEM((peers, block, columns), jnp.bfloat16),
            pltpu.VMEM((fh, rows, 1), jnp.float32),
            pltpu.VMEM((fh, rows, 1), jnp.float32),
            pltpu.VMEM((fh, rows, fd), jnp.float32),
            dma((peers,)),
            dma((peers,)),
            dma,
            dma((n,)),
            dma((n,)),
            dma((n,)),
            dma((n,)),
            dma((peers * pieces,)),
            dma((peers * pieces,)),
        ]
        + gather_sems(5)
        + gather_sems(2),
        compiler_params=pltpu.CompilerParams(
            collective_id=0, has_side_effects=True, vmem_limit_bytes=56 * 1024 * 1024
        ),
        name="layer",
    )(
        tokens,
        norm_gain[None, :],
        ret_query_weight.T,
        ret_key_weight.T,
        ret_value_weight,
        fox_query_weight,
        fox_key_weight,
        fox_value_weight,
        ret_decay,
        ret_state,
        head_norm_gain[None, :],
        fox_gates.T,
        ret_out_weight,
        fox_out_weight,
    )


def solution(mesh):
    placed = (
        P(("grp", "sp"), "tp"),
        P(),
        P("sp", "tp"),
        P("sp", "tp"),
        P("sp", "tp"),
        P("sp", "tp"),
        P("sp", "tp"),
        P("sp", "tp"),
        P("tp"),
        P(("grp", "tp"), None, None),
        P("tp"),
        P("grp", "tp"),
        P("tp", "sp"),
        P("tp", "sp"),
    )
    body = functools.partial(local, mesh.shape["sp"], mesh.shape["tp"], mesh.shape["grp"])
    return jax.shard_map(
        body, mesh=mesh, in_specs=placed, out_specs=P(("grp", "sp", "tp"), None), check_vma=False
    )
```

time: 68.3 us -> 63.5 us (0.930); the launches traced: 68.1 us -> 62.6 us
  local copies, waits for them, and re-layouts: 6.26 us -> 1.67 us
  Pallas kernels: 61.6 us -> 60.9 us
    unnamed x32 -> x1, local copies, waits for them, and re-layouts: 5.95 us -> 1.67 us
    pallas_call x1, Pallas kernels: 61.6 us -> 60.9 us  [local(): pl.pallas_call(functools.partial(kernel, size), out_shape=jax.ShapeDtypeS...]
where the time goes in v2:
time: 63.5 us; the launch traced here: 62.6 us
  Pallas kernels  60.9 us (96%)
  local copies, waits for them, and re-layouts  1.67 us (3%)
    pallas_call x1, Pallas kernels, local(): pl.pallas_call(functools.partial(kernel, size), out_shape=jax.ShapeDtypeS...  60.9 us
    unnamed x1, local copies, waits for them, and re-layouts  1.67 us

profile of v2, /device:TPU:24, one launch (start us, length us, event | category | flops | bytes accessed | tf_op | source)
XLA Modules:
  0.0 62.6 jit_solution(10012473678872530480)
XLA Ops:
  0.0 60.9 %layer.1 = bf16[64,2048]{1,0:T(8,128)(2,1)} custom-call(bf16[256,512]{1,0:T(8,128)(2,1)} %tok_ref.1, f32[1,2048]{1,0:T(1,128)} %bitcast.7, bf16[64,512]{1,0:T(8,128)(2,1)} %bitcast.5, bf16[64,512]{1,0:T(8,128)(2,1)} %bitcast.6, bf16[512,128]{1,0:T(8,128)(2,1)} %wrv_ref.1, bf16[512,128]{1,0:T(8,128)(2,1)} %wfq_ref.1, bf16[512,128]{1,0:T(8,128)(2,1)} %wfk_ref.1, ...), custom_call_target="tpu_custom_call" | custom-call | tf_op jit(solution)/shard_map/layer/pallas_call | solution.py:515
  60.9 1.7 %copy.16 = bf16[64,2048]{1,0:T(8,128)(2,1)} copy(bf16[64,2048]{1,0:T(8,128)(2,1)} %layer.1) | data formatting | bytes 524288

commit v3 on v2

--- a/solution.py
+++ b/solution.py
@@ -154,6 +154,8 @@
     sum_buf,
     mix_buf,
     rs_send,
+    pair_buf,
+    pair_sum,
     rs_buf,
     top_buf,
     total_buf,
@@ -165,6 +167,8 @@
     kv_r,
     sum_s,
     sum_r,
+    pair_s,
+    pair_r,
     rs_s,
     rs_r,
     *gather_sems,
@@ -173,6 +177,7 @@
     me, t, g = lax.axis_index("sp"), lax.axis_index("tp"), lax.axis_index("grp")
     rows, feats = tok_ref.shape
     owns = [wfk_ref, wfv_ref, wfq_ref, wrv_ref, qk_own]
+    early = 2
     starts = [0]
     for own in owns:
         starts.append(starts[-1] + own.shape[1])
@@ -192,8 +197,12 @@
         start = pl.multiple_of(src * out_cols + first, count)
         return wout_buf.at[pl.ds(start, count), c * depth : (c + 1) * depth]
 
-    weights = LineGather(owns, weight_place, gather_sems[:6], n, n_grp, me, g)
-    outs = LineGather([ret_out_ref, fox_out_ref], out_place, gather_sems[6:], n, n_grp, me, g)
+    def late_place(src, c, first, count):
+        return weight_place(src, c + early, first, count)
+
+    firsts = LineGather(owns[:early], weight_place, gather_sems[:6], n, n_grp, me, g)
+    lasts = LineGather(owns[early:], late_place, gather_sems[6:12], n, n_grp, me, g)
+    outs = LineGather([ret_out_ref, fox_out_ref], out_place, gather_sems[12:], n, n_grp, me, g)
 
     barrier = pltpu.get_barrier_semaphore()
 
@@ -227,18 +236,22 @@
         src = lax.rem(t + n_tp - d, n_tp)
         return rdma(tok_ref, tok_buf.at[src], tok_s.at[d - 1], tok_r.at[d - 1], tp=src)
 
-    weights.start()
+    firsts.start()
     tok_local = pltpu.make_async_copy(tok_ref, tok_buf.at[t], tok_loc)
     for d in range(1, n_tp):
         tok_copy(d).start()
     tok_local.start()
 
-    def weight_step(k, _):
-        weights.relay(k)
+    def first_step(k, _):
+        firsts.relay(k)
+
+        @pl.when(k == 1)
+        def _():
+            lasts.start()
+
         return 0
 
-    lax.fori_loop(1, n, weight_step, 0)
-    outs.start()
+    lax.fori_loop(1, n, first_step, 0)
 
     tok_local.wait()
     for d in range(1, n_tp):
@@ -259,18 +272,34 @@
     def sum_copy(src):
         return rdma(sum_buf.at[src], sum_buf.at[src], sum_s.at[src], sum_r.at[src], sp=jnp.minimum(me + 1, n - 1))
 
-    weights.arrive((0, 1))
+    firsts.arrive((0, 1))
     kv_buf[me] = jnp.dot(
         norm_buf[...], w_buf[:, : starts[2]], preferred_element_type=jnp.float32
     ).astype(jnp.bfloat16)
 
+    def kv_forward(k):
+        src = me - k
+
+        @pl.when(src >= 0)
+        def _():
+            kv_copy(src).wait_recv()
+
+            @pl.when(has_up)
+            def _():
+                kv_copy(src).start()
+
     @pl.when(has_up)
     def _():
         kv_copy(me).start()
 
-    if n > 1:
-        outs.relay(1)
-    weights.arrive((2, 3, 4))
+    def last_step(k, _):
+        lasts.relay(k)
+        kv_forward(k)
+        return 0
+
+    lax.fori_loop(1, n, last_step, 0)
+    outs.start()
+    lasts.arrive((0, 1, 2))
     proj_buf[...] = jnp.dot(
         norm_buf[...], w_buf[:, starts[2] :], preferred_element_type=jnp.float32
     ).astype(jnp.bfloat16)
@@ -332,18 +361,14 @@
 
         @pl.when(src >= 0)
         def _():
-            kv_copy(src).wait_recv()
-
-            @pl.when(has_up)
-            def _():
-                kv_copy(src).start()
-
             sum_copy(src).wait_recv()
 
             @pl.when(has_up)
             def _():
                 sum_copy(src).start()
 
+    if n > 1:
+        outs.relay(1)
     attend(me, True)
 
     offset = (me * rows).astype(jnp.float32)
@@ -391,55 +416,82 @@
         mix_buf[:, cols] = (weighted_buf[h] / total_buf[h]).astype(jnp.bfloat16)
 
     block = rows // n_tp
-    columns = rs_send.shape[1]
+    columns = pair_buf.shape[1]
     wide = out_cols if direct else columns
     pieces = columns // wide
-    mine = pl.ds(pl.multiple_of(t * block, block), block)
+    half = n_tp // 2
+    parity, pair = lax.rem(t, 2), lax.div(t, 2)
+
+    def piece_cols(piece):
+        return pl.ds(pl.multiple_of(piece * wide, wide), wide)
+
+    def slot(at):
+        return pl.ds(pl.multiple_of(at * block, block), block)
+
+    def pair_copy(piece):
+        cols = piece_cols(piece)
+        return rdma(
+            rs_send.at[1 - parity, :, cols],
+            pair_buf.at[:, cols],
+            pair_s.at[piece],
+            pair_r.at[piece],
+            tp=t + 1 - 2 * parity,
+        )
 
     def rs_copy(d, piece):
-        to = lax.rem(t + d, n_tp)
-        cols = pl.ds(pl.multiple_of(piece * wide, wide), wide)
+        to = lax.rem(pair + d, half)
+        cols = piece_cols(piece)
         at = (d - 1) * pieces + piece
         return rdma(
-            rs_send.at[pl.ds(pl.multiple_of(to * block, block), block), cols],
-            rs_buf.at[d - 1, :, cols],
-            rs_s.at[at],
-            rs_r.at[at],
-            tp=to,
+            pair_sum.at[slot(to), cols], rs_buf.at[d - 1, :, cols], rs_s.at[at], rs_r.at[at], tp=2 * to + parity
         )
 
     def project(piece):
-        cols = pl.ds(pl.multiple_of(piece * wide, wide), wide)
+        cols = piece_cols(piece)
         if direct:
             value = jnp.dot(mix_buf[...], wout_buf[:, cols], preferred_element_type=jnp.float32)
         else:
             value = lax.dot_general(mix_buf[...], wout_buf[...], NT, preferred_element_type=jnp.float32)
-        rs_send[:, cols] = value.astype(jnp.bfloat16)
-        for d in range(1, n_tp):
+        value = value.astype(jnp.bfloat16)
+        for b in range(n_tp):
+            at = slice(b // 2 * block, (b // 2 + 1) * block)
+            rs_send[b % 2, at, cols] = value[b * block : (b + 1) * block]
+        pair_copy(piece).start()
+
+    def reduce(piece):
+        cols = piece_cols(piece)
+        pair_copy(piece).wait_recv()
+        both = rs_send[parity, :, cols].astype(jnp.float32) + pair_buf[:, cols].astype(jnp.float32)
+        pair_sum[:, cols] = both.astype(jnp.bfloat16)
+        for d in range(1, half):
             rs_copy(d, piece).start()
+
+    def order(i):
+        falling = jnp.where(i <= me, me - i, i)
+        rising = jnp.where(i <= n - 1 - me, me + i, n - 1 - i)
+        return jnp.where(2 * me >= n, falling, rising)
 
     if direct:
         for c in range(2):
             outs.local(c).wait()
         project(me)
 
-        def out_step(k, _):
-            for src in (me - k, me + k):
-
-                @pl.when((src >= 0) & (src < n))
-                def _(src=src):
-                    outs.arrive_shard(src, (0, 1))
-                    project(src)
-
+        def out_step(i, _):
+            outs.arrive_shard(order(i), (0, 1))
+            project(order(i))
+            reduce(order(i - 1))
             return 0
 
         lax.fori_loop(1, n, out_step, 0)
+        reduce(order(jnp.int32(n - 1)))
     else:
         outs.arrive((0, 1))
         project(0)
-
-    summed = rs_send[mine, :].astype(jnp.float32)
-    for d in range(1, n_tp):
+        reduce(0)
+
+    own = slot(pair)
+    summed = rs_send[parity, own, :].astype(jnp.float32) + pair_buf[own, :].astype(jnp.float32)
+    for d in range(1, half):
         for piece in range(pieces):
             rs_copy(d, piece).wait_recv()
         summed = summed + rs_buf[d - 1].astype(jnp.float32)
@@ -447,9 +499,12 @@
 
     for d in range(1, n_tp):
         tok_copy(d).wait_send()
-        for piece in range(pieces):
+    for piece in range(pieces):
+        pair_copy(piece).wait_send()
+        for d in range(1, half):
             rs_copy(d, piece).wait_send()
-    weights.finish()
+    firsts.finish()
+    lasts.finish()
     outs.finish()
 
     @pl.when(has_up)
@@ -511,6 +566,7 @@
     size = (n, n_tp, n_grp, hr, dk, vd, fh, fd, direct)
     block = rows // n_tp
     peers = max(n_tp - 1, 1)
+    far = max(n_tp // 2 - 1, 1)
     pieces = n if direct else 1
     return pl.pallas_call(
         functools.partial(kernel, size),
@@ -527,8 +583,10 @@
             pltpu.VMEM((n, rows, 2 * fh * fd), jnp.bfloat16),
             pltpu.VMEM((n, hr, dk, vd), jnp.float32),
             pltpu.VMEM((rows, 2 * depth), jnp.bfloat16),
-            pltpu.VMEM((rows, columns), jnp.bfloat16),
-            pltpu.VMEM((peers, block, columns), jnp.bfloat16),
+            pltpu.VMEM((2, rows // 2, columns), jnp.bfloat16),
+            pltpu.VMEM((rows // 2, columns), jnp.bfloat16),
+            pltpu.VMEM((rows // 2, columns), jnp.bfloat16),
+            pltpu.VMEM((far, block, columns), jnp.bfloat16),
             pltpu.VMEM((fh, rows, 1), jnp.float32),
             pltpu.VMEM((fh, rows, 1), jnp.float32),
             pltpu.VMEM((fh, rows, fd), jnp.float32),
@@ -539,13 +597,16 @@
             dma((n,)),
             dma((n,)),
             dma((n,)),
-            dma((peers * pieces,)),
-            dma((peers * pieces,)),
+            dma((pieces,)),
+            dma((pieces,)),
+            dma((far * pieces,)),
+            dma((far * pieces,)),
         ]
-        + gather_sems(5)
+        + gather_sems(2)
+        + gather_sems(3)
         + gather_sems(2),
         compiler_params=pltpu.CompilerParams(
-            collective_id=0, has_side_effects=True, vmem_limit_bytes=56 * 1024 * 1024
+            collective_id=0, has_side_effects=True, vmem_limit_bytes=32 * 1024 * 1024
         ),
         name="layer",
     )(

time: 63.5 us -> 72.2 us (1.14)
  the two profiles are of different devices: /device:TPU:24 before, /device:TPU:0 now
where the time goes in v3:
time: 72.2 us; the launch traced here: 71.7 us
  Pallas kernels  60.8 us (84%)
  local copies, waits for them, and re-layouts  10.9 us (15%)
    pallas_call x1, Pallas kernels, local(): pl.pallas_call(functools.partial(kernel, size), out_shape=jax.ShapeDtypeS...  60.8 us
    unnamed x29, local copies, waits for them, and re-layouts  10.9 us

profile of v3, /device:TPU:0, one launch (start us, length us, event | category | flops | bytes accessed | tf_op | source)
XLA Modules:
  0.0 71.7 jit_solution(1427381843372483360)
XLA Ops:
  0.0 0.0 copy-start.10
  0.0 0.0 copy-start.12
  0.0 0.0 copy-start.13
  0.0 0.7 copy-done.10
  0.7 0.0 copy-done.12
  0.7 0.0 copy-done.13
  0.7 0.0 copy-start
  0.7 0.9 %copy-done = bf16[256,512]{1,0:T(8,128)(2,1)S(1)} copy-done((bf16[256,512]{1,0:T(8,128)(2,1)S(1)}, bf16[256,512]{1,0:T(8,128)(2,1)}, u32[]{:S(2)}) %copy-start) | copy-done | bytes 262168
  1.7 0.0 copy-start.1
  1.7 0.9 %copy-done.1 = bf16[512,128]{1,0:T(8,128)(2,1)S(1)} copy-done((bf16[512,128]{1,0:T(8,128)(2,1)S(1)}, bf16[512,128]{1,0:T(8,128)(2,1)}, u32[]{:S(2)}) %copy-start.1) | copy-done | bytes 131096
  2.6 0.0 copy-start.2
  2.6 0.9 %copy-done.2 = bf16[512,128]{1,0:T(8,128)(2,1)S(1)} copy-done((bf16[512,128]{1,0:T(8,128)(2,1)S(1)}, bf16[512,128]{1,0:T(8,128)(2,1)}, u32[]{:S(2)}) %copy-start.2) | copy-done | bytes 131096
  3.5 0.0 copy-start.3
  3.5 0.9 %copy-done.3 = bf16[512,128]{1,0:T(8,128)(2,1)S(1)} copy-done((bf16[512,128]{1,0:T(8,128)(2,1)S(1)}, bf16[512,128]{1,0:T(8,128)(2,1)}, u32[]{:S(2)}) %copy-start.3) | copy-done | bytes 131096
  4.4 0.0 copy-start.4
  4.4 0.9 %copy-done.4 = bf16[512,128]{1,0:T(8,128)(2,1)S(1)} copy-done((bf16[512,128]{1,0:T(8,128)(2,1)S(1)}, bf16[512,128]{1,0:T(8,128)(2,1)}, u32[]{:S(2)}) %copy-start.4) | copy-done | bytes 131096
  5.3 0.0 copy-start.5
  5.3 0.9 %copy-done.5 = bf16[128,512]{1,0:T(8,128)(2,1)S(1)} copy-done((bf16[128,512]{1,0:T(8,128)(2,1)S(1)}, bf16[128,512]{1,0:T(8,128)(2,1)}, u32[]{:S(2)}) %copy-start.5) | copy-done | bytes 131096
  6.2 0.0 copy-start.6
  6.2 0.9 %copy-done.6 = bf16[128,512]{1,0:T(8,128)(2,1)S(1)} copy-done((bf16[128,512]{1,0:T(8,128)(2,1)S(1)}, bf16[128,512]{1,0:T(8,128)(2,1)}, u32[]{:S(2)}) %copy-start.6) | copy-done | bytes 131096
  7.1 0.0 copy-start.7
  7.1 0.8 %copy-done.7 = bf16[512,64]{0,1:T(8,128)(2,1)S(1)} copy-done((bf16[512,64]{0,1:T(8,128)(2,1)S(1)}, bf16[512,64]{0,1:T(8,128)(2,1)}, u32[]{:S(2)}) %copy-start.7) | copy-done | bytes 65560
  7.9 0.0 copy-start.8
  7.9 0.8 %copy-done.8 = bf16[512,64]{0,1:T(8,128)(2,1)S(1)} copy-done((bf16[512,64]{0,1:T(8,128)(2,1)S(1)}, bf16[512,64]{0,1:T(8,128)(2,1)}, u32[]{:S(2)}) %copy-start.8) | copy-done | bytes 65560
  8.8 0.0 copy-start.9
  8.8 0.8 %copy-done.9 = f32[2,32,64]{2,1,0:T(8,128)S(1)} copy-done((f32[2,32,64]{2,1,0:T(8,128)S(1)}, f32[2,32,64]{2,1,0:T(8,128)}, u32[]{:S(2)}) %copy-start.9) | copy-done | bytes 16408
  9.5 0.0 copy-start.11
  9.5 0.7 copy-done.11
  10.2 60.8 %layer.1 = bf16[64,2048]{1,0:T(8,128)(2,1)S(1)} custom-call(bf16[256,512]{1,0:T(8,128)(2,1)S(1)} %copy-done, f32[1,2048]{1,0:T(1,128)S(1)} %bitcast.7, bf16[64,512]{1,0:T(8,128)(2,1)S(1)} %bitcast.5, bf16[64,512]{1,0:T(8,128)(2,1)S(1)} %bitcast.6, bf16[512,128]{1,0:T(8,128)(2,1)S(1)} %copy-done.1, bf16[512,128]{1,0:T(8,128)(2,1)S(1)} %copy-done.2, ...), custom_call_target="tpu_custom_call" | custom-call | tf_op jit(solution)/shard_map/layer/pallas_call | solution.py:571
  71.0 0.7 copy.16
Async XLA Ops:
  0.0 0.7 copy-start.10
  0.0 0.7 copy-start.12
  0.0 0.7 copy-start.13
  0.7 1.0 %copy-start = (bf16[256,512]{1,0:T(8,128)(2,1)S(1)}, bf16[256,512]{1,0:T(8,128)(2,1)}, u32[]{:S(2)}) copy-start(bf16[256,512]{1,0:T(8,128)(2,1)} %tok_ref.1) | copy-start | bytes 786436
  1.7 0.9 %copy-start.1 = (bf16[512,128]{1,0:T(8,128)(2,1)S(1)}, bf16[512,128]{1,0:T(8,128)(2,1)}, u32[]{:S(2)}) copy-start(bf16[512,128]{1,0:T(8,128)(2,1)} %wrv_ref.1) | copy-start | bytes 393220
  2.6 0.9 %copy-start.2 = (bf16[512,128]{1,0:T(8,128)(2,1)S(1)}, bf16[512,128]{1,0:T(8,128)(2,1)}, u32[]{:S(2)}) copy-start(bf16[512,128]{1,0:T(8,128)(2,1)} %wfq_ref.1) | copy-start | bytes 393220
  3.5 0.9 %copy-start.3 = (bf16[512,128]{1,0:T(8,128)(2,1)S(1)}, bf16[512,128]{1,0:T(8,128)(2,1)}, u32[]{:S(2)}) copy-start(bf16[512,128]{1,0:T(8,128)(2,1)} %wfk_ref.1) | copy-start | bytes 393220
  4.4 0.9 %copy-start.4 = (bf16[512,128]{1,0:T(8,128)(2,1)S(1)}, bf16[512,128]{1,0:T(8,128)(2,1)}, u32[]{:S(2)}) copy-start(bf16[512,128]{1,0:T(8,128)(2,1)} %wfv_ref.1) | copy-start | bytes 393220
  5.3 0.9 %copy-start.5 = (bf16[128,512]{1,0:T(8,128)(2,1)S(1)}, bf16[128,512]{1,0:T(8,128)(2,1)}, u32[]{:S(2)}) copy-start(bf16[128,512]{1,0:T(8,128)(2,1)} %ret_out_ref.1) | copy-start | bytes 393220
  6.2 0.9 %copy-start.6 = (bf16[128,512]{1,0:T(8,128)(2,1)S(1)}, bf16[128,512]{1,0:T(8,128)(2,1)}, u32[]{:S(2)}) copy-start(bf16[128,512]{1,0:T(8,128)(2,1)} %fox_out_ref.1) | copy-start | bytes 393220
  7.1 0.8 %copy-start.7 = (bf16[512,64]{0,1:T(8,128)(2,1)S(1)}, bf16[512,64]{0,1:T(8,128)(2,1)}, u32[]{:S(2)}) copy-start(bf16[512,64]{0,1:T(8,128)(2,1)} %param.16) | copy-start | bytes 196612
  7.9 0.8 %copy-start.8 = (bf16[512,64]{0,1:T(8,128)(2,1)S(1)}, bf16[512,64]{0,1:T(8,128)(2,1)}, u32[]{:S(2)}) copy-start(bf16[512,64]{0,1:T(8,128)(2,1)} %param.17) | copy-start | bytes 196612
  8.8 0.8 %copy-start.9 = (f32[2,32,64]{2,1,0:T(8,128)S(1)}, f32[2,32,64]{2,1,0:T(8,128)}, u32[]{:S(2)}) copy-start(f32[2,32,64]{2,1,0:T(8,128)} %state_ref.1) | copy-start | bytes 49156
  9.5 0.7 copy-start.11

commit v4 on v3

--- a/solution.py
+++ b/solution.py
@@ -237,6 +237,7 @@
         return rdma(tok_ref, tok_buf.at[src], tok_s.at[d - 1], tok_r.at[d - 1], tp=src)
 
     firsts.start()
+    lasts.start()
     tok_local = pltpu.make_async_copy(tok_ref, tok_buf.at[t], tok_loc)
     for d in range(1, n_tp):
         tok_copy(d).start()
@@ -245,13 +246,11 @@
     def first_step(k, _):
         firsts.relay(k)
 
-        @pl.when(k == 1)
-        def _():
-            lasts.start()
-
+        lasts.relay(k)
         return 0
 
     lax.fori_loop(1, n, first_step, 0)
+    outs.start()
 
     tok_local.wait()
     for d in range(1, n_tp):
@@ -292,13 +291,7 @@
     def _():
         kv_copy(me).start()
 
-    def last_step(k, _):
-        lasts.relay(k)
-        kv_forward(k)
-        return 0
-
-    lax.fori_loop(1, n, last_step, 0)
-    outs.start()
+    outs.relay(1)
     lasts.arrive((0, 1, 2))
     proj_buf[...] = jnp.dot(
         norm_buf[...], w_buf[:, starts[2] :], preferred_element_type=jnp.float32
@@ -367,8 +360,6 @@
             def _():
                 sum_copy(src).start()
 
-    if n > 1:
-        outs.relay(1)
     attend(me, True)
 
     offset = (me * rows).astype(jnp.float32)
@@ -376,11 +367,13 @@
 
     def step(k, entering):
         src = me - k
+        kv_forward(k)
         forward(k)
 
         @pl.when(k + 1 < n)
         def _():
             outs.relay(k + 1)
+
 
         @pl.when(src >= 0)
         def _():
@@ -606,7 +599,7 @@
         + gather_sems(3)
         + gather_sems(2),
         compiler_params=pltpu.CompilerParams(
-            collective_id=0, has_side_effects=True, vmem_limit_bytes=32 * 1024 * 1024
+            collective_id=0, has_side_effects=True, vmem_limit_bytes=56 * 1024 * 1024
         ),
         name="layer",
     )(

time: 72.2 us -> 59.8 us (0.83)
  the two profiles are of different devices: /device:TPU:0 before, /device:TPU:24 now
where the time goes in v4:
time: 59.8 us; the launch traced here: 59.2 us
  Pallas kernels  57.5 us (96%)
  local copies, waits for them, and re-layouts  1.67 us (3%)
    pallas_call x1, Pallas kernels, local(): pl.pallas_call(functools.partial(kernel, size), out_shape=jax.ShapeDtypeS...  57.5 us
    unnamed x1, local copies, waits for them, and re-layouts  1.67 us

profile of v4, /device:TPU:24, one launch (start us, length us, event | category | flops | bytes accessed | tf_op | source)
XLA Modules:
  0.0 59.2 jit_solution(13496924155989551722)
XLA Ops:
  0.0 57.5 %layer.1 = bf16[64,2048]{1,0:T(8,128)(2,1)} custom-call(bf16[256,512]{1,0:T(8,128)(2,1)} %tok_ref.1, f32[1,2048]{1,0:T(1,128)} %bitcast.7, bf16[64,512]{1,0:T(8,128)(2,1)} %bitcast.5, bf16[64,512]{1,0:T(8,128)(2,1)} %bitcast.6, bf16[512,128]{1,0:T(8,128)(2,1)} %wrv_ref.1, bf16[512,128]{1,0:T(8,128)(2,1)} %wfq_ref.1, bf16[512,128]{1,0:T(8,128)(2,1)} %wfk_ref.1, ...), custom_call_target="tpu_custom_call" | custom-call | tf_op jit(solution)/shard_map/layer/pallas_call | solution.py:564
  57.5 1.7 %copy.16 = bf16[64,2048]{1,0:T(8,128)(2,1)} copy(bf16[64,2048]{1,0:T(8,128)(2,1)} %layer.1) | data formatting | bytes 524288
